TPU v7x, 32 devices: a whole 2x2x4 slice. The times are simulated.
32 devices in a mesh: kv: 8 (over z, y), tp: 4 (over x, core).
Axes of the slice: x: 2, y: 2, z: 4, core: 2. Of those that a mesh axis runs over, the one named last changes fastest.
Arguments:
- tokens: bfloat16 [32, 4096], P(None, 'kv'), may hold values from -40 to 40, as said below
- norm_gain: float32 [4096], P('kv'), may hold values from 0.1 to 1.9
- w_query: bfloat16 [4096, 2048], P('kv', 'tp'), may hold values from -0.09375 to 0.09375
- w_key: bfloat16 [4096, 512], P('kv', 'tp'), may hold values from -0.09375 to 0.09375
- w_value: bfloat16 [4096, 512], P('kv', 'tp'), may hold values from -0.09375 to 0.09375
- forget_weight: bfloat16 [4096, 32], replicated, may hold values from -0.09375 to 0.09375
- forget_bias: float32 [32], P('tp'), may hold values from -1 to 3
- kv_cache: bfloat16 [32, 10240, 8, 128], P(None, 'kv', 'tp'), may hold values from -6 to 6
- cum_gates: float32 [32, 32, 10240], P(None, 'tp', 'kv'), may hold values from -10500 to 0, as said below
- lengths: int32 [32], replicated, may hold values from 1 to 10240, as said below
- w_out: bfloat16 [2048, 4096], P('tp', 'kv'), may hold values from -0.25 to 0.25
Outputs:
- mixed: bfloat16 [32, 4096], P(None, 'kv')
- log_weight: float32 [32, 32], P(None, 'tp')
Inputs may be any that keep to these rules, and one draw needn't show every extreme that they name: Columns of tokens come in 16 groups of equal width. `cum_gates`: each row does not rise along the positions. `lengths`: some sequence has all 10240 positions cached.
All inputs are finite; a program needn't handle non-finite values.
Results may differ from a plain program's by a relative error of at most 0.0307.
Values may be sent and summed in bfloat16 or wider, within the bound.
No kernel may reach another device: no remote copies, remote signals or barrier semaphores. Data moves between devices by JAX's collectives and lax.ppermute only.
A program may use at most 128 MiB of HBM per device.

v0:
```python
import jax
import jax.numpy as jnp
from jax import lax
from jax.sharding import PartitionSpec as P

norm_eps = 1e-05
masked_floor = -1e30


def finish_rows(row_squares, sum_query, sum_keyval, sum_gate, forget_bias, model_width):
    row_scale = lax.rsqrt(row_squares / model_width + norm_eps)[:, None]
    query = (row_scale * sum_query).astype(jnp.bfloat16)
    keyval = (row_scale * sum_keyval).astype(jnp.bfloat16)
    log_gate = jax.nn.log_sigmoid(row_scale * sum_gate + forget_bias)
    return (query, keyval, log_gate)


def shards(
    tokens,
    norm_gain,
    w_query,
    w_key,
    w_value,
    forget_weight,
    forget_bias,
    kv_cache,
    cum_gates,
    lengths,
    w_out,
):
    rows_count, col_count = tokens.shape
    span_len = kv_cache.shape[1]
    kv_local = kv_cache.shape[2]
    head_size = kv_cache.shape[3] // 2
    heads_local = cum_gates.shape[1]
    group_size = heads_local // kv_local
    model_width = col_count * lax.axis_size("kv")
    tokens_f = tokens.astype(jnp.float32)
    squares = jnp.sum(tokens_f * tokens_f, axis=1)
    normalized_input = (tokens_f * norm_gain).astype(jnp.bfloat16)
    gate_cols = lax.dynamic_slice(
        forget_weight,
        (lax.axis_index("kv") * col_count, lax.axis_index("tp") * heads_local),
        (col_count, heads_local),
    )
    part_query = jnp.dot(normalized_input, w_query, preferred_element_type=jnp.float32)
    part_keyval = jnp.concatenate(
        [
            jnp.dot(normalized_input, w_key, preferred_element_type=jnp.float32),
            jnp.dot(normalized_input, w_value, preferred_element_type=jnp.float32),
        ],
        axis=1,
    )
    part_gate = jnp.dot(normalized_input, gate_cols, preferred_element_type=jnp.float32)
    total_sq, sum_query, sum_keyval, sum_gate = (
        lax.psum(squares.astype(jnp.bfloat16), "kv").astype(jnp.float32),
        lax.psum(part_query.astype(jnp.bfloat16), "kv").astype(jnp.float32),
        lax.psum(part_keyval.astype(jnp.bfloat16), "kv").astype(jnp.float32),
        lax.psum(part_gate.astype(jnp.bfloat16), "kv").astype(jnp.float32),
    )
    query, keyval, log_gate = finish_rows(
        total_sq, sum_query, sum_keyval, sum_gate, forget_bias, model_width
    )
    inv_root = head_size ** (-0.5)
    query_head_rows = query.reshape(rows_count, kv_local, group_size, head_size)
    cached_keys = kv_cache[:, :, :, :head_size]
    cached_vals = kv_cache[:, :, :, head_size:]
    scores = (
        jnp.einsum(
            "bkgd,blkd->bkgl", query_head_rows, cached_keys, preferred_element_type=jnp.float32
        )
        * inv_root
    )
    biased = scores - cum_gates.reshape(rows_count, kv_local, group_size, span_len)
    first_pos = lax.axis_index("kv") * span_len
    positions = first_pos + lax.iota(jnp.int32, span_len)
    in_range = positions[None, :] < lengths[:, None]
    last_pos = lengths - 1
    holds_last = (last_pos >= first_pos) & (last_pos < first_pos + span_len)
    last_index = jnp.clip(last_pos - first_pos, 0, span_len - 1)
    last_cum = jnp.take_along_axis(
        cum_gates, jnp.broadcast_to(last_index[:, None, None], (rows_count, heads_local, 1)), axis=2
    )[:, :, 0]
    cum_query = last_cum + log_gate
    fresh_key_row = keyval[:, : kv_local * head_size].reshape(rows_count, kv_local, head_size)
    value_new = keyval[:, kv_local * head_size :].reshape(rows_count, kv_local, head_size)
    new_biased = (
        jnp.einsum(
            "pnof,pnf->pno", query_head_rows, fresh_key_row, preferred_element_type=jnp.float32
        )
        * inv_root
    )
    new_biased = new_biased - cum_query.reshape(rows_count, kv_local, group_size)
    range_mask = in_range[:, None, None, :]
    owner_mask = holds_last[:, None, None]
    peak_local = jnp.max(jnp.where(range_mask, biased, masked_floor), axis=-1)
    peak_local = jnp.where(owner_mask, jnp.maximum(peak_local, new_biased), peak_local)
    weights = jnp.where(range_mask, jnp.exp(biased - peak_local[..., None]), 0.0)
    new_weight = jnp.where(owner_mask, jnp.exp(new_biased - peak_local), 0.0)
    weight_sum = jnp.sum(weights, axis=-1) + new_weight
    weighted = jnp.einsum(
        "bkgl,blkd->bkgd",
        weights.astype(jnp.bfloat16),
        cached_vals,
        preferred_element_type=jnp.float32,
    )
    weighted = (
        weighted
        + new_weight.astype(jnp.bfloat16).astype(jnp.float32)[..., None]
        * value_new.astype(jnp.float32)[:, :, None, :]
    )
    anchor = jnp.where(holds_last[:, None], cum_query, 0.0).reshape(
        rows_count, kv_local, group_size
    )
    peak = lax.pmax(peak_local, "kv")
    rescale_factor = jnp.exp(peak_local - peak)
    weight_sum, weighted, anchor = lax.psum(
        (weight_sum * rescale_factor, weighted * rescale_factor[..., None], anchor), "kv"
    )
    attended = (
        (weighted / weight_sum[..., None])
        .astype(jnp.bfloat16)
        .reshape(rows_count, heads_local * head_size)
    )
    log_weight = (peak + jnp.log(weight_sum) + anchor).reshape(rows_count, heads_local)
    part_out = jnp.dot(attended, w_out, preferred_element_type=jnp.float32)
    mixed = lax.psum(part_out.astype(jnp.bfloat16), "tp")
    return (mixed, log_weight)


def solution(mesh):
    placed = (
        P(None, "kv"),
        P("kv"),
        P("kv", "tp"),
        P("kv", "tp"),
        P("kv", "tp"),
        P(),
        P("tp"),
        P(None, "kv", "tp", None),
        P(None, "tp", "kv"),
        P(),
        P("tp", "kv"),
    )
    return jax.shard_map(
        shards,
        mesh=mesh,
        in_specs=placed,
        out_specs=(P(None, "kv"), P(None, "tp")),
        check_vma=False,
    )
```

profile of v0, /device:TPU:0, one launch (start us, length us, event | category | flops | bytes accessed | tf_op | source)
XLA Modules:
  0.0 224.6 jit_solution(18268263765218162662)
XLA Ops:
  7.2 0.0 copy-start
  7.2 0.0 all-reduce.4.cloned.1.call-start
  7.2 0.0 copy-start.2
  7.3 41.6 %fusion.40 = (bf16[32,1280,2,64]{3,2,1,0:T(2,128)(2,1)}, bf16[32,1280,2,64]{3,2,1,0:T(2,128)(2,1)}) fusion(bf16[32,1280,2,128]{3,2,1,0:T(2,128)(2,1)} %param.18), kind=kLoop, calls=%fused_computation.64 | loop fusion | bytes 41943040 | tf_op jit(solution)/shard_map/slice | solution.py:66
  48.9 0.0 copy-start.3
  48.9 0.0 copy-start.7
  48.9 0.0 copy-start.6
  48.9 0.0 copy-start.8
  48.9 1.5 reshape.198
  50.4 0.1 fusion.22
  50.5 0.2 convolution_convert_fusion.1
  50.7 0.1 convolution_convert_fusion.2
  50.9 0.0 copy-done.6
  50.9 0.1 convolution_convert_fusion.3
  51.0 0.8 convolution_convert_fusion.4
  51.8 39.3 %all-reduce.1 = (bf16[32,512]{1,0:T(8,128)(2,1)S(1)}, bf16[32]{0:T(256)(128)(2,1)S(1)}, bf16[32,8]{0,1:T(8,128)(2,1)S(1)}, bf16[32,256]{1,0:T(8,128)(2,1)S(1)}) all-reduce(bf16[32,512]{1,0:T(8,128)(2,1)S(1)} %convolution_convert_fusion.1, bf16[32]{0:T(256)(128)(2,1)S(1)} %fusion.22, ...), channel_id=1, replica_groups=mesh['kv'=8,'tp'=4] {'kv'}, use_global_device_ids=true, to_apply=%region_2.0 | all-reduce | flops 24864 | bytes 99456 | tf_op jit(solution)/shard_map/psum | solution.py:57
  91.2 0.1 multiply_convert_fusion
  91.3 0.1 reshape.197
  91.4 0.1 broadcast_compare_fusion
  91.5 12.1 %select_reduce_fusion = (f32[32,2,4]{2,1,0:T(2,128)S(1)}, f32[32,2,4,1280]{3,2,1,0:T(4,128)S(1)}) fusion(pred[32,1280]{1,0:T(8,128)(4,1)S(1)} %broadcast_compare_fusion, f32[32,2,4,1280]{3,2,1,0:T(4,128)} %reshape.198, bf16[32,2,4,64]{3,2,1,0:T(4,128)(2,1)S(1)} %reshape.197, bf16[32,1280,2,64]{3,2,1,0:T(2,128)(2,1)} %get-tuple-element.15), kind=kOutput, calls=%fused_computation.8 | convolution fusion | flops 43253504 | bytes 13181952 | tf_op jit(solution)/shard_map/bkgd,blkd->bkgl/dot_general | solution.py:69
  103.6 0.1 copy.42
  103.8 0.1 copy.40
  103.9 0.1 reshape.207
  104.0 2.3 %gather_fusion = f32[256]{0:T(256)S(1)} fusion(f32[32,8,1280]{2,1,0:T(8,128)S(1)} %copy-done.2, s32[256]{0:T(256)S(1)} %reshape.207), kind=kCustom, calls=%fused_computation | custom fusion | bytes 5120 | tf_op jit(solution)/shard_map/jit(take_along_axis)/gather | solution.py:81
  106.2 0.1 gather.7
  106.3 0.1 copy.41
  106.4 0.1 multiply_convert_fusion.1
  106.5 0.1 reshape.218
  106.6 0.2 fusion.41
  106.8 0.1 copy.51
  106.9 0.1 broadcast_select_fusion
  107.0 0.1 copy.44
  107.1 17.1 %pmax.7 = f32[32,2,4]{0,2,1:T(4,128)S(1)} all-reduce(f32[32,2,4]{0,2,1:T(4,128)S(1)} %maximum_select_fusion), channel_id=1, replica_groups=mesh['kv'=8,'tp'=4] {'kv'}, use_global_device_ids=true, to_apply=%region_6.7 | all-reduce | flops 256 | bytes 2048 | tf_op jit(solution)/shard_map/pmax | solution.py:115
  124.2 0.8 fusion.16
  125.0 0.1 copy.48
  125.1 0.1 copy.47
  125.2 0.1 reshape.204
  125.3 0.1 copy.46
  125.4 10.7 %fusion.13 = f32[32,2,4,64]{3,2,1,0:T(4,128)} fusion(bf16[32,1280,2,64]{3,2,1,0:T(2,128)(2,1)} %get-tuple-element.16, f32[32,2,4,1280]{3,2,1,0:T(4,128)S(1)} %get-tuple-element.21, f32[32,2,4]{2,1,0:T(2,128)S(1)} %copy.44, pred[32,1280]{1,0:T(8,128)(4,1)S(1)} %broadcast_compare_fusion, f32[32,2,4]{2,1,0:T(2,128)S(1)} %copy.47, ...), kind=kOutput, calls=%fused_computation.10 | convolution fusion | flops 42975232 | bytes 11922432 | tf_op jit(solution)/shard_map/bkgl,blkd->bkgd/dot_general | solution.py:101
  136.2 0.0 all-reduce.4.cloned.1.call-update
  136.2 19.6 %all-reduce = (f32[32,2,4]{0,2,1:T(4,128)S(1)}, f32[32,2,4]{0,2,1:T(4,128)S(1)}) all-reduce(f32[32,2,4]{0,2,1:T(4,128)S(1)} %get-tuple-element.10, f32[32,2,4]{0,2,1:T(4,128)S(1)} %bitcast.31), channel_id=1, replica_groups=mesh['kv'=8,'tp'=4] {'kv'}, use_global_device_ids=true, to_apply=%region_9.10 | all-reduce | flops 512 | bytes 4096 | tf_op jit(solution)/shard_map/psum | solution.py:117
  155.8 0.6 add_add_fusion
  156.4 0.1 copy.49
  156.5 49.0 %all-reduce.4.cloned.1.call-done = f32[32,2,4,64]{3,2,1,0:T(4,128)} async-done(((f32[32,2,4,64]{3,2,1,0:T(4,128)}), f32[32,2,4,64]{3,2,1,0:T(4,128)}) %all-reduce.4.cloned.1.call-update) | async-done | bytes 65552 | tf_op jit(solution)/shard_map/psum | solution.py:117
  205.5 1.0 divide_convert_fusion
  206.5 0.1 reshape.201
  206.7 0.2 convolution_convert_fusion
  206.9 10.9 %psum.62 = bf16[32,512]{1,0:T(8,128)(2,1)} all-reduce(bf16[32,512]{1,0:T(8,128)(2,1)S(1)} %convolution_convert_fusion), channel_id=1, replica_groups=mesh['kv'=8,'tp'=4] {'tp'}, use_global_device_ids=true, to_apply=%region_10.11 | all-reduce | flops 16384 | bytes 65536 | tf_op jit(solution)/shard_map/psum | solution.py:127
  (26 shorter events, 0.1 us)
Async XLA Ops:
  7.2 43.3 %copy-start = (bf16[512,512]{1,0:T(8,128)(2,1)S(1)}, bf16[512,512]{1,0:T(8,128)(2,1)}, u32[]{:S(2)}) copy-start(bf16[512,512]{1,0:T(8,128)(2,1)} %param.13) | copy-start | bytes 1572868
  7.2 198.3 %all-reduce.4.cloned.1.call-start = ((), (), s32[]{:S(2)}) async-start(), calls=%async_computation | async-start | bytes 262144 | tf_op jit(solution)/shard_map/psum | solution.py:117
  7.2 41.6 %copy-start.2 = (f32[32,8,1280]{2,1,0:T(8,128)S(1)}, f32[32,8,1280]{2,1,0:T(8,128)}, u32[]{:S(2)}) copy-start(f32[32,8,1280]{2,1,0:T(8,128)} %param.19) | copy-start | bytes 3932164
  48.9 1.5 copy-start.3
  48.9 1.6 copy-start.7
  48.9 1.8 copy-start.5
  48.9 2.0 copy-start.6
  48.9 42.5 %copy-start.8 = (s32[32]{0:T(128)S(1)}, s32[32]{0:T(128)}, u32[]{:S(2)}) copy-start(s32[32]{0:T(128)} %param.20) | copy-start | bytes 388
  103.9 2.9 %copy-start.9 = (f32[8]{0:T(128)S(1)}, f32[8]{0:T(128)}, u32[]{:S(2)}) copy-start(f32[8]{0:T(128)} %param.17) | copy-start | bytes 100
  125.4 81.3 %copy-start.4 = (bf16[512,512]{1,0:T(8,128)(2,1)S(1)}, bf16[512,512]{1,0:T(8,128)(2,1)}, u32[]{:S(2)}) copy-start(bf16[512,512]{1,0:T(8,128)(2,1)} %param.21) | copy-start | bytes 1572868
  125.4 92.3 %copy-start.1 = (bf16[512,512]{1,0:T(8,128)(2,1)S(1)}, bf16[512,512]{1,0:T(8,128)(2,1)}, u32[]{:S(2)}) copy-start(bf16[512,512]{1,0:T(8,128)(2,1)} %param.13) | copy-start | bytes 1572868
Sparse Core Ops, SparseCore 0:
  136.3 69.1 all-reduce.3
where the time goes:
time: 225 us
  blocking collectives  86.9 us (39%)
  waiting for transfers between devices  49 us (22%)
  local copies, waits for them, and re-layouts  46.8 us (21%)
  matrix products  24.5 us (11%)
  between operations  14.3 us (6%)
  other arithmetic  2.95 us (1%)
    psum x1, waiting for transfers between devices, shards(): lax.psum((weight_sum * rescale_factor, weighted * rescale_factor[..., Non...  49 us
    slice x1, local copies, waits for them, and re-layouts, shards(): cached_keys = kv_cache[:, :, :, :head_size]  41.6 us
    psum x1, blocking collectives, shards(): lax.psum(part_query.astype(jnp.bfloat16), 'kv').astype(jnp.float32)  39.3 us
    psum x1, blocking collectives, shards(): lax.psum((weight_sum * rescale_factor, weighted * rescale_factor[..., Non...  19.6 us
    pmax x1, blocking collectives, shards(): peak = lax.pmax(peak_local, 'kv')  17.1 us
    dot_general x1, matrix products, shards(): jnp.einsum('bkgd,blkd->bkgl', query_head_rows, cached_keys, preferred_ele...  12.1 us
    psum x1, blocking collectives, shards(): mixed = lax.psum(part_out.astype(jnp.bfloat16), 'tp')  10.9 us
    dot_general x1, matrix products, shards(): jnp.einsum('bkgl,blkd->bkgd', weights.astype(jnp.bfloat16), cached_vals,...  10.7 us
  transfers between devices with their start and end apart: 1, of which 1 were waited for; matrix products, arithmetic and copies ran while one was open for 0% of the time, Pallas kernels for 0%

commit v1 on v0

v1 whole, which is shorter than its diff:
```python
import functools

import jax
import jax.numpy as jnp
from jax import lax
from jax.experimental import pallas as pl
from jax.experimental.pallas import tpu as pltpu
from jax.sharding import PartitionSpec as P

norm_eps = 1e-05
masked_floor = -1e30
lanes = 128


def rounded(x):
    return x.astype(jnp.bfloat16).astype(jnp.float32)


def xor_permute(x, axis, step):
    size = lax.axis_size(axis)
    return lax.ppermute(x, axis, [(i, i ^ step) for i in range(size)])


def exchange_sum(x, axis):
    step = 1
    while step < lax.axis_size(axis):
        mine = lax.optimization_barrier(x.astype(jnp.bfloat16))
        other = xor_permute(mine, axis, step)
        x = mine.astype(jnp.float32) + other.astype(jnp.float32)
        step *= 2
    return x


def expand_body(rel_ref, cum_ref, bias_ref, last_ref, *, kv_local, group):
    rows, heads, span = cum_ref.shape
    wide = lanes * kv_local
    half = span * kv_local // 2
    spread = (
        lax.broadcasted_iota(jnp.int32, (lanes, wide), 1) // kv_local
        == lax.broadcasted_iota(jnp.int32, (lanes, wide), 0)
    ).astype(jnp.bfloat16)
    spread2 = jnp.concatenate([spread, spread], axis=0)
    col = lax.broadcasted_iota(jnp.int32, (heads, wide), 1)
    row_head = lax.broadcasted_iota(jnp.int32, (heads, wide), 0) // group
    own = col % kv_local == row_head
    local = col // kv_local
    narrow = lax.broadcasted_iota(jnp.int32, (heads, lanes), 1)
    base = pl.program_id(0) * rows
    last = [jnp.zeros((heads, lanes), jnp.float32) for _ in range(rows)]
    for c in range(span // lanes):
        x = cum_ref[:, :, c * lanes : (c + 1) * lanes].reshape(rows * heads, lanes)
        high = rounded(x)
        mid = rounded(x - high)
        low = (x - high - mid).astype(jnp.bfloat16)
        pair = jnp.concatenate([high.astype(jnp.bfloat16), mid.astype(jnp.bfloat16)], axis=1)
        y = jnp.dot(pair, spread2, preferred_element_type=jnp.float32) + jnp.dot(
            low, spread, preferred_element_type=jnp.float32
        )
        start = c * wide
        side = start // half
        start = start - side * half
        for r in range(rows):
            rel = rel_ref[base + r] - c * lanes
            ok = own & (local < rel)
            bias_ref[r, side * heads : (side + 1) * heads, start : start + wide] = jnp.where(
                ok, y[r * heads : (r + 1) * heads], -masked_floor
            )
            last[r] = last[r] + jnp.where(
                narrow == rel - 1, x[r * heads : (r + 1) * heads], 0.0
            )
    for r in range(rows):
        last_ref[r] = jnp.broadcast_to(jnp.sum(last[r], axis=1, keepdims=True), (heads, lanes))


def expand_gates(rel_len, cum_gates, kv_local, group):
    batch, heads, span = cum_gates.shape
    rows = 8
    half = span * kv_local // 2
    return pl.pallas_call(
        functools.partial(expand_body, kv_local=kv_local, group=group),
        grid_spec=pltpu.PrefetchScalarGridSpec(
            num_scalar_prefetch=1,
            grid=(batch // rows,),
            in_specs=[pl.BlockSpec((rows, heads, span), lambda i, rel: (i, 0, 0))],
            out_specs=[
                pl.BlockSpec((rows, 2 * heads, half), lambda i, rel: (i, 0, 0)),
                pl.BlockSpec((rows, heads, lanes), lambda i, rel: (i, 0, 0)),
            ],
        ),
        out_shape=[
            jax.ShapeDtypeStruct((batch, 2 * heads, half), jnp.float32),
            jax.ShapeDtypeStruct((batch, heads, lanes), jnp.float32),
        ],
        name="expand_gates",
    )(rel_len, cum_gates)


def attend_body(query_ref, cache_ref, bias_ref, out_ref, *, scale):
    rows, length, width = cache_ref.shape
    heads = query_ref.shape[1] // 2
    half = length // 2
    lane = lax.broadcasted_iota(jnp.int32, (heads, width), 1)
    for r in range(rows):
        both = jnp.concatenate([cache_ref[r, :half], cache_ref[r, half:]], axis=1)
        scores = lax.dot_general(
            query_ref[r], both, (((1,), (1,)), ((), ())), preferred_element_type=jnp.float32
        )
        biased = scores * scale - bias_ref[r]
        peak = jnp.max(biased, axis=1, keepdims=True)
        peak = jnp.maximum(jnp.maximum(peak[:heads], peak[heads:]), masked_floor)
        weights = jnp.exp(biased - jnp.concatenate([peak, peak], axis=0))
        total = jnp.sum(weights, axis=1, keepdims=True)
        total = total[:heads] + total[heads:]
        values = jnp.dot(weights.astype(jnp.bfloat16), both, preferred_element_type=jnp.float32)
        values = values[:heads, :width] + values[heads:, width:]
        out_ref[r] = jnp.where(lane == 0, peak, jnp.where(lane == 1, total, values))


def attend(query, cache, bias, scale):
    batch, length, width = cache.shape
    rows = 4
    heads = query.shape[1] // 2

    def spec(*shape):
        return pl.BlockSpec((rows,) + shape, lambda i: (i, 0, 0))

    return pl.pallas_call(
        functools.partial(attend_body, scale=scale),
        grid=(batch // rows,),
        in_specs=[
            spec(2 * heads, 2 * width),
            spec(length, width),
            spec(2 * heads, length // 2),
        ],
        out_specs=spec(heads, width),
        out_shape=jax.ShapeDtypeStruct((batch, heads, width), jnp.float32),
        name="attend",
    )(query, cache, bias)


def read_field(stats, index, heads):
    parts = [
        pltpu.roll(stats, (lanes - (3 * index + t) * heads) % lanes, 1) for t in range(3)
    ]
    return parts[0] + (parts[1] + parts[2])


def write_field(x, index, heads):
    high = rounded(x)
    mid = rounded(x - high)
    low = rounded(x - high - mid)
    out = 0.0
    for t, part in enumerate((high, mid, low)):
        out = out + pltpu.roll(part, (3 * index + t) * heads, 1)
    return out


def spread_factors(factors, heads, head_size):
    width = heads * head_size
    stacked = jnp.concatenate(factors, axis=0)
    high = rounded(stacked)
    pair = jnp.concatenate(
        [high.astype(jnp.bfloat16), (stacked - high).astype(jnp.bfloat16)], axis=1
    )
    spread = (
        lax.broadcasted_iota(jnp.int32, (2 * lanes, width), 1) // head_size
        == lax.broadcasted_iota(jnp.int32, (2 * lanes, width), 0) % lanes
    ).astype(jnp.bfloat16)
    wide = jnp.dot(pair, spread, preferred_element_type=jnp.float32)
    rows = factors[0].shape[0]
    return [wide[i * rows : (i + 1) * rows] for i in range(len(factors))]


def merge_stats(mine_ref, other_ref, heads, width):
    own_stats = mine_ref[:, width:].astype(jnp.float32)
    far_stats = other_ref[:, width:].astype(jnp.float32)
    used = lax.broadcasted_iota(jnp.int32, own_stats.shape, 1) < heads
    own_peak, far_peak = (read_field(s, 0, heads) for s in (own_stats, far_stats))
    own_sum, far_sum = (read_field(s, 1, heads) for s in (own_stats, far_stats))
    anchor = read_field(own_stats, 2, heads) + read_field(far_stats, 2, heads)
    own_peak, far_peak, anchor, own_sum, far_sum = (
        jnp.where(used, x, 0.0) for x in (own_peak, far_peak, anchor, own_sum, far_sum)
    )
    peak = jnp.maximum(own_peak, far_peak)
    own_factor = jnp.exp(own_peak - peak)
    far_factor = jnp.exp(far_peak - peak)
    total = own_sum * own_factor + far_sum * far_factor
    return used, peak, total, anchor, own_factor, far_factor


def merge_body(mine_ref, other_ref, out_ref, *, heads, head_size):
    width = heads * head_size
    used, peak, total, anchor, own_factor, far_factor = merge_stats(
        mine_ref, other_ref, heads, width
    )
    own_wide, far_wide = spread_factors(
        [jnp.where(used, own_factor, 0.0), jnp.where(used, far_factor, 0.0)], heads, head_size
    )
    values = own_wide * mine_ref[:, :width].astype(jnp.float32) + far_wide * other_ref[
        :, :width
    ].astype(jnp.float32)
    out_ref[:, :width] = values.astype(jnp.bfloat16)
    stats = (
        write_field(peak, 0, heads)
        + write_field(jnp.where(used, total, 0.0), 1, heads)
        + write_field(anchor, 2, heads)
    )
    out_ref[:, width:] = stats.astype(jnp.bfloat16)


def merge(mine, other, heads, head_size):
    return pl.pallas_call(
        functools.partial(merge_body, heads=heads, head_size=head_size),
        out_shape=jax.ShapeDtypeStruct(mine.shape, mine.dtype),
        name="merge",
    )(mine, other)


def finish_body(
    mine_ref, other_ref, fresh_ref, value_ref, attended_ref, log_ref, *, heads, head_size
):
    width = heads * head_size
    used, peak, total, anchor, own_factor, far_factor = merge_stats(
        mine_ref, other_ref, heads, width
    )
    fresh = fresh_ref[...]
    cum_query = anchor + pltpu.roll(fresh, lanes - heads, 1)
    fresh_biased = jnp.where(used, fresh - cum_query, 0.0)
    top = jnp.maximum(peak, fresh_biased)
    keep = jnp.exp(peak - top)
    fresh_weight = jnp.exp(fresh_biased - top)
    total = jnp.where(used, total * keep + fresh_weight, 1.0)
    factors = [own_factor * keep / total, far_factor * keep / total, rounded(fresh_weight) / total]
    own_wide, far_wide, fresh_wide = spread_factors(
        [jnp.where(used, f, 0.0) for f in factors], heads, head_size
    )
    values = (
        own_wide * mine_ref[:, :width].astype(jnp.float32)
        + far_wide * other_ref[:, :width].astype(jnp.float32)
        + fresh_wide * value_ref[...].astype(jnp.float32)
    )
    attended_ref[...] = values.astype(jnp.bfloat16)
    log_ref[...] = top + jnp.log(total) + cum_query


def finish(mine, other, fresh, value, heads, head_size):
    batch = mine.shape[0]
    return pl.pallas_call(
        functools.partial(finish_body, heads=heads, head_size=head_size),
        out_shape=[
            jax.ShapeDtypeStruct((batch, heads * head_size), jnp.bfloat16),
            jax.ShapeDtypeStruct((batch, lanes), jnp.float32),
        ],
        name="finish",
    )(mine, other, fresh, value)


def split_three(x):
    high = lax.reduce_precision(x, 8, 7)
    mid = lax.reduce_precision(x - high, 8, 7)
    low = lax.reduce_precision(x - high - mid, 8, 7)
    return [high, mid, low]


def shards(
    tokens,
    norm_gain,
    w_query,
    w_key,
    w_value,
    forget_weight,
    forget_bias,
    kv_cache,
    cum_gates,
    lengths,
    w_out,
):
    batch, cols = tokens.shape
    span = kv_cache.shape[1]
    kv_local = kv_cache.shape[2]
    head_size = kv_cache.shape[3] // 2
    heads = cum_gates.shape[1]
    group = heads // kv_local
    width = heads * head_size
    kv_width = kv_local * head_size
    model_width = cols * lax.axis_size("kv")

    first_pos = lax.axis_index("kv") * span
    bias, last_cum = expand_gates(lengths - first_pos, cum_gates, kv_local, group)

    tokens_f = tokens.astype(jnp.float32)
    squares = jnp.sum(tokens_f * tokens_f, axis=1, keepdims=True)
    normed = (tokens_f * norm_gain).astype(jnp.bfloat16)
    gate_cols = lax.dynamic_slice(
        forget_weight,
        (lax.axis_index("kv") * cols, lax.axis_index("tp") * heads),
        (cols, heads),
    )
    parts = [
        jnp.dot(normed, w, preferred_element_type=jnp.float32)
        for w in (w_query, w_key, w_value, gate_cols)
    ]
    parts.append(squares)
    used = sum(p.shape[1] for p in parts)
    parts.append(jnp.zeros((batch, -used % lanes), jnp.float32))
    sums = exchange_sum(jnp.concatenate(parts, axis=1), "kv")

    edge = width + 2 * kv_width
    row_scale = lax.rsqrt(sums[:, edge + heads : edge + heads + 1] / model_width + norm_eps)
    projected = (row_scale * sums[:, :edge]).astype(jnp.bfloat16)
    query = projected[:, :width]
    log_gate = jax.nn.log_sigmoid(row_scale * sums[:, edge : edge + heads] + forget_bias)
    query_rows = query.reshape(batch, heads, head_size)
    full = 4 * head_size
    query_pair = jnp.concatenate(
        [
            jnp.pad(query_rows, ((0, 0), (0, 0), (0, full - head_size))),
            jnp.pad(query_rows, ((0, 0), (0, 0), (full // 2, full // 2 - head_size))),
        ],
        axis=1,
    )
    scale = head_size ** (-0.5)
    cache = kv_cache.reshape(batch, span * kv_local, 2 * head_size)
    partial = attend(query_pair, cache, bias, scale)

    key_rows = projected[:, width : width + kv_width].reshape(batch, kv_local, 1, head_size)
    fresh_score = jnp.sum(
        query.reshape(batch, kv_local, group, head_size).astype(jnp.float32)
        * key_rows.astype(jnp.float32),
        axis=-1,
    ).reshape(batch, heads)
    fresh = jnp.concatenate(
        [
            fresh_score * scale,
            log_gate,
            jnp.zeros((batch, lanes - 2 * heads), jnp.float32),
        ],
        axis=1,
    )
    value_rows = projected[:, width + kv_width :].reshape(batch, kv_local, 1, head_size)
    value_wide = jnp.broadcast_to(value_rows, (batch, kv_local, group, head_size)).reshape(
        batch, width
    )

    stats = split_three(partial[:, :, 0]) + split_three(partial[:, :, 1])
    stats = stats + split_three(last_cum[:, :, 0])
    stats.append(jnp.zeros((batch, lanes - 9 * heads), jnp.float32))
    packed = jnp.concatenate(
        [partial[:, :, head_size:].reshape(batch, width)] + stats, axis=1
    ).astype(jnp.bfloat16)

    step = 1
    while 2 * step < lax.axis_size("kv"):
        packed = merge(packed, xor_permute(packed, "kv", step), heads, head_size)
        step *= 2
    attended, log_weight = finish(
        packed, xor_permute(packed, "kv", step), fresh, value_wide, heads, head_size
    )
    part_out = jnp.dot(attended, w_out, preferred_element_type=jnp.float32)
    mixed = exchange_sum(part_out, "tp").astype(jnp.bfloat16)
    return (mixed, log_weight[:, :heads])


def solution(mesh):
    placed = (
        P(None, "kv"),
        P("kv"),
        P("kv", "tp"),
        P("kv", "tp"),
        P("kv", "tp"),
        P(),
        P("tp"),
        P(None, "kv", "tp", None),
        P(None, "tp", "kv"),
        P(),
        P("tp", "kv"),
    )
    return jax.shard_map(
        shards,
        mesh=mesh,
        in_specs=placed,
        out_specs=(P(None, "kv"), P(None, "tp")),
        check_vma=False,
    )
```

time: 225 us -> 81.5 us (0.36)
  blocking collectives: 86.9 us -> 0 us
  local copies, waits for them, and re-layouts: 46.8 us -> 10.5 us
  waiting for transfers between devices: 49 us -> 13.8 us
  Pallas kernels: 0 us -> 31.8 us
  matrix products: 24.5 us -> 4.96 us
  starting transfers between devices: 0.04 us -> 14.1 us
  between operations: 14.3 us -> 0.83 us
    psum x3 -> x0, blocking collectives: 69.8 us -> none  [the longest x1 39.3 us: shards(): lax.psum(part_query.astype(jnp.bfloat16), 'kv').astype(jnp.float32)]
    psum x1 -> x0, waiting for transfers between devices: 49 us -> none  [shards(): lax.psum((weight_sum * rescale_factor, weighted * rescale_factor[..., Non...]
    slice x1 -> x2, local copies, waits for them, and re-layouts: 41.6 us -> 2.11 us  [the longest x1 1.07 us: shards(): stats = split_three(partial[:, :, 0]) + split_three(partial[:, :, 1])]
    pallas_call x0 -> x5, Pallas kernels: none -> 31.8 us  [the longest x1 21.5 us: attend(): pl.pallas_call(functools.partial(attend_body, scale=scale), grid=(batch /...]
    dot_general x7 -> x4, matrix products: 24.3 us -> 4.02 us  [shards(): jnp.dot(normed, w, preferred_element_type=jnp.float32)]
    pmax x1 -> x0, blocking collectives: 17.1 us -> none  [shards(): peak = lax.pmax(peak_local, 'kv')]
    ppermute x0 -> x8, starting transfers between devices: none -> 14.1 us  [xor_permute(): return lax.ppermute(x, axis, [(i, i ^ step) for i in range(size)])]
    ppermute x0 -> x8, waiting for transfers between devices: none -> 13.8 us  [xor_permute(): return lax.ppermute(x, axis, [(i, i ^ step) for i in range(size)])]
  transfers between devices with their start and end apart: 1 -> 8, of which waited for: 1 -> 7; matrix products, arithmetic and copies ran while one was open for 0% -> 9% of each run, Pallas kernels for 0% -> 7%
where the time goes in v1:
time: 81.5 us; the launch traced here: 80.7 us
  Pallas kernels  31.8 us (39%)
  starting transfers between devices  14.1 us (17%)
  waiting for transfers between devices  13.8 us (17%)
  local copies, waits for them, and re-layouts  10.5 us (13%)
  matrix products  4.96 us (6%)
  other arithmetic  4.78 us (6%)
  between operations  0.83 us (1%)
    pallas_call x1, Pallas kernels, attend(): pl.pallas_call(functools.partial(attend_body, scale=scale), grid=(batch /...  21.5 us
    ppermute x8, starting transfers between devices, xor_permute(): return lax.ppermute(x, axis, [(i, i ^ step) for i in range(size)])  14.1 us
    ppermute x8, waiting for transfers between devices, xor_permute(): return lax.ppermute(x, axis, [(i, i ^ step) for i in range(size)])  13.8 us
    pallas_call x1, Pallas kernels, expand_gates(): pl.pallas_call(functools.partial(expand_body, kv_local=kv_local, group=gr...  5.33 us
    dot_general x4, matrix products, shards(): jnp.dot(normed, w, preferred_element_type=jnp.float32)  4.02 us
    unnamed x17, local copies, waits for them, and re-layouts  3.72 us
    pallas_call x2, Pallas kernels, merge(): pl.pallas_call(functools.partial(merge_body, heads=heads, head_size=head_...  3.28 us
    pallas_call x1, local copies, waits for them, and re-layouts, expand_gates(): pl.pallas_call(functools.partial(expand_body, kv_local=kv_local, group=gr...  2.74 us
  transfers between devices with their start and end apart: 8, of which 7 were waited for; matrix products, arithmetic and copies ran while one was open for 9% of the time, Pallas kernels for 7%

profile of v1, /device:TPU:0, one launch (start us, length us, event | category | flops | bytes accessed | tf_op | source)
XLA Modules:
  0.0 80.7 jit_solution(12654905298507050626)
XLA Ops:
  0.7 0.9 %fusion.5 = bf16[32]{0:T(256)(128)(2,1)S(1)} fusion(bf16[32,512]{1,0:T(8,128)(2,1)} %param.11), kind=kLoop, calls=%fused_computation.20 | loop fusion | flops 49120 | bytes 32832 | tf_op jit(solution)/shard_map/reduce_sum | solution.py:292
  1.6 0.9 %convolution_convert_fusion.4 = bf16[32,8]{0,1:T(8,128)(2,1)S(1)} fusion(bf16[32,512]{1,0:T(8,128)(2,1)} %param.11, f32[512]{0:T(512)} %param.12, bf16[4096,32]{0,1:T(8,128)(2,1)} %param.16, s32[]{:T(128)S(6)} %select_n.11, s32[]{:T(128)S(6)} %select_n.12), kind=kOutput, calls=%fused_computation.4 | convolution fusion | flops 311552 | bytes 43528 | tf_op jit(solution)/shard_map/dot_general | solution.py:300
  2.5 0.1 copy.34
  2.6 0.1 copy.35
  2.7 1.1 %convolution_convert_fusion.3 = bf16[32,128]{1,0:T(8,128)(2,1)S(1)} fusion(bf16[512,128]{1,0:T(8,128)(2,1)} %param.14, bf16[32,512]{1,0:T(8,128)(2,1)} %param.11, f32[512]{0:T(512)} %param.12), kind=kOutput, calls=%fused_computation.3 | convolution fusion | flops 4247552 | bytes 174080 | tf_op jit(solution)/shard_map/dot_general | solution.py:300
  3.8 1.1 %convolution_convert_fusion.2 = bf16[32,128]{1,0:T(8,128)(2,1)S(1)} fusion(bf16[512,128]{1,0:T(8,128)(2,1)} %param.15, bf16[32,512]{1,0:T(8,128)(2,1)} %param.11, f32[512]{0:T(512)} %param.12), kind=kOutput, calls=%fused_computation.2 | convolution fusion | flops 4247552 | bytes 174080 | tf_op jit(solution)/shard_map/dot_general | solution.py:300
  4.9 0.9 %convolution_convert_fusion.1 = bf16[32,512]{1,0:T(8,128)(2,1)S(1)} fusion(bf16[512,512]{1,0:T(8,128)(2,1)S(1)} %copy-done, bf16[32,512]{1,0:T(8,128)(2,1)} %param.11, f32[512]{0:T(512)} %param.12), kind=kOutput, calls=%fused_computation.1 | convolution fusion | flops 16842752 | bytes 591872 | tf_op jit(solution)/shard_map/dot_general | solution.py:300
  5.8 0.1 concatenate.14
  5.9 3.1 %collective-permute-start = (bf16[32,896]{1,0:T(8,128)(2,1)S(1)}, bf16[32,896]{1,0:T(8,128)(2,1)S(1)}, u32[]{:S(2)}, u32[]{:S(2)}) collective-permute-start(bf16[32,896]{1,0:T(8,128)(2,1)S(1)} %concatenate.14), channel_id=1, source_target_pairs={{0,4},{4,0},{8,12},{12,8},{16,20},{20,16},{24,28},{28,24},{1,5},{5... | collective-permute-start | bytes 172040 | tf_op jit(solution)/shard_map/ppermute | solution.py:21
  9.0 2.2 %collective-permute-done = bf16[32,896]{1,0:T(8,128)(2,1)S(1)} collective-permute-done((bf16[32,896]{1,0:T(8,128)(2,1)S(1)}, bf16[32,896]{1,0:T(8,128)(2,1)S(1)}, u32[]{:S(2)}, u32[]{:S(2)}) %collective-permute-start) | collective-permute-done | bytes 57376 | tf_op jit(solution)/shard_map/ppermute | solution.py:21
  11.2 2.1 %collective-permute-start.1 = (bf16[32,896]{1,0:T(8,128)(2,1)S(1)}, bf16[32,896]{1,0:T(8,128)(2,1)S(1)}, u32[]{:S(2)}, u32[]{:S(2)}) collective-permute-start(bf16[32,896]{1,0:T(8,128)(2,1)S(1)} %add_convert_fusion.1), channel_id=1, source_target_pairs={{0,8},{4,12},{8,0},{12,4},{16,24},{20,28},{24,16},{28,20},{1,9},{5... | collective-permute-start | bytes 172040 | tf_op jit(solution)/shard_map/ppermute | solution.py:21
  13.3 1.2 %broadcast_subtract_fusion.rel_ref = s32[32]{0:T(128)} fusion(s32[32]{0:T(128)} %param.20, s32[]{:T(128)S(6)} %mul.63), kind=kLoop, calls=%fused_computation.56 | loop fusion | flops 32 | bytes 260 | tf_op jit(solution)/shard_map/sub | solution.py:289
  14.5 5.3 %expand_gates.1 = (f32[32,16,1280]{2,1,0:T(8,128)}, f32[32,8,128]{2,1,0:T(8,128)}) custom-call(s32[32]{0:T(128)} %broadcast_subtract_fusion.rel_ref, f32[32,8,1280]{2,1,0:T(8,128)} %cum_ref.1), custom_call_target="tpu_custom_call" | custom-call | tf_op jit(solution)/shard_map/expand_gates/pallas_call | solution.py:79
  19.8 2.7 %copy.38 = f32[32,8,128]{1,0,2:T(8,128)S(1)} copy(f32[32,8,128]{2,1,0:T(8,128)} %get-tuple-element.7) | data formatting | bytes 262144 | tf_op jit(solution)/shard_map/expand_gates/pallas_call | solution.py:79
  22.6 2.7 %collective-permute-start.2 = (bf16[32,896]{1,0:T(8,128)(2,1)S(1)}, bf16[32,896]{1,0:T(8,128)(2,1)S(1)}, u32[]{:S(2)}, u32[]{:S(2)}) collective-permute-start(bf16[32,896]{1,0:T(8,128)(2,1)S(1)} %add_convert_fusion), channel_id=1, source_target_pairs={{0,16},{4,20},{8,24},{12,28},{16,0},{20,4},{24,8},{28,12},{1,17},{... | collective-permute-start | bytes 172040 | tf_op jit(solution)/shard_map/ppermute | solution.py:21
  25.3 2.6 %collective-permute-done.2 = bf16[32,896]{1,0:T(8,128)(2,1)S(1)} collective-permute-done((bf16[32,896]{1,0:T(8,128)(2,1)S(1)}, bf16[32,896]{1,0:T(8,128)(2,1)S(1)}, u32[]{:S(2)}, u32[]{:S(2)}) %collective-permute-start.2) | collective-permute-done | bytes 57376 | tf_op jit(solution)/shard_map/ppermute | solution.py:21
  27.9 0.2 fusion.21
  28.2 0.1 reshape.37
  28.3 0.7 fusion.2.query_ref
  29.1 21.5 %attend.1 = f32[32,8,128]{2,1,0:T(8,128)} custom-call(bf16[32,16,256]{2,1,0:T(8,128)(2,1)} %fusion.2.query_ref, bf16[32,2560,128]{2,1,0:T(8,128)(2,1)} %bitcast.35, f32[32,16,1280]{2,1,0:T(8,128)} %get-tuple-element.6.bias_ref), custom_call_target="tpu_custom_call" | custom-call | tf_op jit(solution)/shard_map/attend/pallas_call | solution.py:127
  50.5 1.0 %slice.84 = bf16[32,8,64]{2,1,0:T(8,128)(2,1)S(1)} slice(f32[32,8,128]{2,1,0:T(8,128)} %attend.1), slice={[0:32], [0:8], [64:128]} | slice | bytes 65536 | tf_op jit(solution)/shard_map/slice | solution.py:349
  51.6 1.1 %fusion.23 = (f32[32,8,1]{2,1,0:T(8,128)S(1)}, f32[32,8,1]{2,1,0:T(8,128)S(1)}) fusion(f32[32,8,128]{2,1,0:T(8,128)} %attend.1), kind=kLoop, calls=%fused_computation.58 | loop fusion | bytes 4096 | tf_op jit(solution)/shard_map/slice | solution.py:345
  52.7 0.1 fusion.16
  52.9 0.1 reshape.41
  53.0 0.1 reshape.39
  53.1 0.2 copy.43
  53.3 0.3 copy.42
  53.6 0.1 concatenate.16.mine_ref
  53.8 1.9 %collective-permute-start.3 = (bf16[32,640]{1,0:T(8,128)(2,1)S(1)}, bf16[32,640]{1,0:T(8,128)(2,1)S(1)}, u32[]{:S(2)}, u32[]{:S(2)}) collective-permute-start(bf16[32,640]{1,0:T(8,128)(2,1)S(1)} %concatenate.16.mine_ref), channel_id=1, source_target_pairs={{0,4},{4,0},{8,12},{12,8},{16,20},{20,16},{24,28},{28,24},{1,5},{5... | collective-permute-start | bytes 122888 | tf_op jit(solution)/shard_map/ppermute | solution.py:21
  55.7 0.2 multiply_reduce_fusion
  55.9 1.9 %collective-permute-done.3.other_ref = bf16[32,640]{1,0:T(8,128)(2,1)S(1)} collective-permute-done((bf16[32,640]{1,0:T(8,128)(2,1)S(1)}, bf16[32,640]{1,0:T(8,128)(2,1)S(1)}, u32[]{:S(2)}, u32[]{:S(2)}) %collective-permute-start.3) | collective-permute-done | bytes 40992 | tf_op jit(solution)/shard_map/ppermute | solution.py:21
  57.8 0.6 copy-done.4
  58.4 1.6 %merge.2.mine_ref = bf16[32,640]{1,0:T(8,128)(2,1)} custom-call(bf16[32,640]{1,0:T(8,128)(2,1)} %copy-done.2, bf16[32,640]{1,0:T(8,128)(2,1)} %copy-done.4), custom_call_target="tpu_custom_call" | custom-call | tf_op jit(solution)/shard_map/merge/pallas_call | solution.py:212
  60.2 4.1 %collective-permute-done.4.other_ref = bf16[32,640]{1,0:T(8,128)(2,1)S(1)} collective-permute-done((bf16[32,640]{1,0:T(8,128)(2,1)}, bf16[32,640]{1,0:T(8,128)(2,1)S(1)}, u32[]{:S(2)}, u32[]{:S(2)}) %collective-permute-start.4) | collective-permute-done | bytes 40992 | tf_op jit(solution)/shard_map/ppermute | solution.py:21
  64.3 0.6 copy-done.5
  64.9 1.6 %merge.3.mine_ref = bf16[32,640]{1,0:T(8,128)(2,1)} custom-call(bf16[32,640]{1,0:T(8,128)(2,1)} %merge.2.mine_ref, bf16[32,640]{1,0:T(8,128)(2,1)} %copy-done.5), custom_call_target="tpu_custom_call" | custom-call | tf_op jit(solution)/shard_map/merge/pallas_call | solution.py:212
  66.5 2.4 %collective-permute-start.5 = (bf16[32,640]{1,0:T(8,128)(2,1)}, bf16[32,640]{1,0:T(8,128)(2,1)S(1)}, u32[]{:S(2)}, u32[]{:S(2)}) collective-permute-start(bf16[32,640]{1,0:T(8,128)(2,1)} %merge.3.mine_ref), channel_id=1, source_target_pairs={{0,16},{4,20},{8,24},{12,28},{16,0},{20,4},{24,8},{28,12},{1,17},{... | collective-permute-start | bytes 122888 | tf_op jit(solution)/shard_map/ppermute | solution.py:21
  69.0 0.7 maximum_maximum_fusion.fresh_ref
  69.8 0.7 reshape.40.value_ref
  70.5 1.2 %collective-permute-done.5.other_ref = bf16[32,640]{1,0:T(8,128)(2,1)S(1)} collective-permute-done((bf16[32,640]{1,0:T(8,128)(2,1)}, bf16[32,640]{1,0:T(8,128)(2,1)S(1)}, u32[]{:S(2)}, u32[]{:S(2)}) %collective-permute-start.5) | collective-permute-done | bytes 40992 | tf_op jit(solution)/shard_map/ppermute | solution.py:21
  71.7 0.6 copy-done.3
  72.3 1.7 %finish.1 = (bf16[32,512]{1,0:T(8,128)(2,1)}, f32[32,128]{1,0:T(8,128)}) custom-call(bf16[32,640]{1,0:T(8,128)(2,1)} %merge.3.mine_ref, bf16[32,640]{1,0:T(8,128)(2,1)} %copy-done.3, f32[32,128]{1,0:T(8,128)} %maximum_maximum_fusion.fresh_ref, bf16[32,512]{1,0:T(8,128)(2,1)} %reshape.40.value_ref), custom_call_target="tpu_custom_call" | custom-call | tf_op jit(solution)/shard_map/finish/pallas_call | solution.py:248
  74.0 0.9 %convolution_convert_fusion = bf16[32,512]{1,0:T(8,128)(2,1)S(1)} fusion(bf16[32,512]{1,0:T(8,128)(2,1)} %get-tuple-element.8, bf16[512,512]{1,0:T(8,128)(2,1)S(1)} %copy-done.1), kind=kOutput, calls=%fused_computation | convolution fusion | flops 16793600 | bytes 589824 | tf_op jit(solution)/shard_map/dot_general | solution.py:359
  74.9 1.2 %collective-permute-done.6 = bf16[32,512]{1,0:T(8,128)(2,1)S(1)} collective-permute-done((bf16[32,512]{1,0:T(8,128)(2,1)S(1)}, bf16[32,512]{1,0:T(8,128)(2,1)S(1)}, u32[]{:S(2)}, u32[]{:S(2)}) %collective-permute-start.6) | collective-permute-done | bytes 32800 | tf_op jit(solution)/shard_map/ppermute | solution.py:21
  76.1 1.9 %collective-permute-start.7 = (bf16[32,512]{1,0:T(8,128)(2,1)S(1)}, bf16[32,512]{1,0:T(8,128)(2,1)S(1)}, u32[]{:S(2)}, u32[]{:S(2)}) collective-permute-start(bf16[32,512]{1,0:T(8,128)(2,1)S(1)} %add_convert_fusion.3), channel_id=1, source_target_pairs={{0,2},{1,3},{2,0},{3,1},{4,6},{5,7},{6,4},{7,5},{8,10},{9,11},{10,... | collective-permute-start | bytes 98312 | tf_op jit(solution)/shard_map/ppermute | solution.py:21
  78.0 1.4 %copy.41 = f32[32,8]{0,1:T(8,128)} copy(f32[32,8]{1,0:T(8,128)} %bitcast.36) | data formatting | bytes 2048
  79.4 0.7 collective-permute-done.7
  80.1 0.6 add_convert_fusion.2
  (33 shorter events, 0.7 us)
Async XLA Ops:
  0.6 4.2 %copy-start = (bf16[512,512]{1,0:T(8,128)(2,1)S(1)}, bf16[512,512]{1,0:T(8,128)(2,1)}, u32[]{:S(2)}) copy-start(bf16[512,512]{1,0:T(8,128)(2,1)} %param.13) | copy-start | bytes 1572868
  5.9 5.2 %collective-permute-start = (bf16[32,896]{1,0:T(8,128)(2,1)S(1)}, bf16[32,896]{1,0:T(8,128)(2,1)S(1)}, u32[]{:S(2)}, u32[]{:S(2)}) collective-permute-start(bf16[32,896]{1,0:T(8,128)(2,1)S(1)} %concatenate.14), channel_id=1, source_target_pairs={{0,4},{4,0},{8,12},{12,8},{16,20},{20,16},{24,28},{28,24},{1,5},{5... | collective-permute-start | bytes 172040 | tf_op jit(solution)/shard_map/ppermute | solution.py:21
  11.2 11.4 %collective-permute-start.1 = (bf16[32,896]{1,0:T(8,128)(2,1)S(1)}, bf16[32,896]{1,0:T(8,128)(2,1)S(1)}, u32[]{:S(2)}, u32[]{:S(2)}) collective-permute-start(bf16[32,896]{1,0:T(8,128)(2,1)S(1)} %add_convert_fusion.1), channel_id=1, source_target_pairs={{0,8},{4,12},{8,0},{12,4},{16,24},{20,28},{24,16},{28,20},{1,9},{5... | collective-permute-start | bytes 172040 | tf_op jit(solution)/shard_map/ppermute | solution.py:21
  22.6 5.3 %collective-permute-start.2 = (bf16[32,896]{1,0:T(8,128)(2,1)S(1)}, bf16[32,896]{1,0:T(8,128)(2,1)S(1)}, u32[]{:S(2)}, u32[]{:S(2)}) collective-permute-start(bf16[32,896]{1,0:T(8,128)(2,1)S(1)} %add_convert_fusion), channel_id=1, source_target_pairs={{0,16},{4,20},{8,24},{12,28},{16,0},{20,4},{24,8},{28,12},{1,17},{... | collective-permute-start | bytes 172040 | tf_op jit(solution)/shard_map/ppermute | solution.py:21
  29.1 23.6 %copy-start.6 = (f32[8]{0:T(128)S(1)}, f32[8]{0:T(128)}, u32[]{:S(2)}) copy-start(f32[8]{0:T(128)} %param.17) | copy-start | bytes 100
  50.5 23.4 %copy-start.1 = (bf16[512,512]{1,0:T(8,128)(2,1)S(1)}, bf16[512,512]{1,0:T(8,128)(2,1)}, u32[]{:S(2)}) copy-start(bf16[512,512]{1,0:T(8,128)(2,1)} %param.21) | copy-start | bytes 1572868
  53.7 4.1 %copy-start.2 = (bf16[32,640]{1,0:T(8,128)(2,1)}, bf16[32,640]{1,0:T(8,128)(2,1)S(1)}, u32[]{:S(2)}) copy-start(bf16[32,640]{1,0:T(8,128)(2,1)S(1)} %concatenate.16.mine_ref) | copy-start | bytes 122884
  53.8 4.1 %collective-permute-start.3 = (bf16[32,640]{1,0:T(8,128)(2,1)S(1)}, bf16[32,640]{1,0:T(8,128)(2,1)S(1)}, u32[]{:S(2)}, u32[]{:S(2)}) collective-permute-start(bf16[32,640]{1,0:T(8,128)(2,1)S(1)} %concatenate.16.mine_ref), channel_id=1, source_target_pairs={{0,4},{4,0},{8,12},{12,8},{16,20},{20,16},{24,28},{28,24},{1,5},{5... | collective-permute-start | bytes 122888 | tf_op jit(solution)/shard_map/ppermute | solution.py:21
  57.8 0.6 copy-start.4
  60.1 4.2 %collective-permute-start.4 = (bf16[32,640]{1,0:T(8,128)(2,1)}, bf16[32,640]{1,0:T(8,128)(2,1)S(1)}, u32[]{:S(2)}, u32[]{:S(2)}) collective-permute-start(bf16[32,640]{1,0:T(8,128)(2,1)} %merge.2.mine_ref), channel_id=1, source_target_pairs={{0,8},{4,12},{8,0},{12,4},{16,24},{20,28},{24,16},{28,20},{1,9},{5... | collective-permute-start | bytes 122888 | tf_op jit(solution)/shard_map/ppermute | solution.py:21
  64.3 0.6 copy-start.5
  66.5 5.1 %collective-permute-start.5 = (bf16[32,640]{1,0:T(8,128)(2,1)}, bf16[32,640]{1,0:T(8,128)(2,1)S(1)}, u32[]{:S(2)}, u32[]{:S(2)}) collective-permute-start(bf16[32,640]{1,0:T(8,128)(2,1)} %merge.3.mine_ref), channel_id=1, source_target_pairs={{0,16},{4,20},{8,24},{12,28},{16,0},{20,4},{24,8},{28,12},{1,17},{... | collective-permute-start | bytes 122888 | tf_op jit(solution)/shard_map/ppermute | solution.py:21
  71.7 0.6 copy-start.3
  74.9 1.2 %collective-permute-start.6 = (bf16[32,512]{1,0:T(8,128)(2,1)S(1)}, bf16[32,512]{1,0:T(8,128)(2,1)S(1)}, u32[]{:S(2)}, u32[]{:S(2)}) collective-permute-start(bf16[32,512]{1,0:T(8,128)(2,1)S(1)} %convolution_convert_fusion), channel_id=1, source_target_pairs={{0,1},{1,0},{2,3},{3,2},{4,5},{5,4},{6,7},{7,6},{8,9},{9,8},{10,11... | collective-permute-start | bytes 98312 | tf_op jit(solution)/shard_map/ppermute | solution.py:21
  76.1 4.0 %collective-permute-start.7 = (bf16[32,512]{1,0:T(8,128)(2,1)S(1)}, bf16[32,512]{1,0:T(8,128)(2,1)S(1)}, u32[]{:S(2)}, u32[]{:S(2)}) collective-permute-start(bf16[32,512]{1,0:T(8,128)(2,1)S(1)} %add_convert_fusion.3), channel_id=1, source_target_pairs={{0,2},{1,3},{2,0},{3,1},{4,6},{5,7},{6,4},{7,5},{8,10},{9,11},{10,... | collective-permute-start | bytes 98312 | tf_op jit(solution)/shard_map/ppermute | solution.py:21

commit v2 on v1

--- a/solution.py
+++ b/solution.py
@@ -95,35 +95,63 @@
     )(rel_len, cum_gates)
 
 
-def attend_body(query_ref, cache_ref, bias_ref, out_ref, *, scale):
+def attend_body(query_ref, cache_ref, bias_ref, last_ref, out_ref, *, scale):
     rows, length, width = cache_ref.shape
     heads = query_ref.shape[1] // 2
     half = length // 2
+    size = width // 2
+
+    def both(r):
+        return jnp.concatenate([cache_ref[r, :half], cache_ref[r, half:]], axis=1)
+
+    biased = [
+        lax.dot_general(
+            query_ref[r], both(r), (((1,), (1,)), ((), ())), preferred_element_type=jnp.float32
+        )
+        * scale
+        - bias_ref[r]
+        for r in range(rows)
+    ]
+    peaks = [jnp.max(x, axis=1, keepdims=True) for x in biased]
+    peaks = [jnp.maximum(jnp.maximum(p[:heads], p[heads:]), masked_floor) for p in peaks]
+    weights = [
+        jnp.exp(x - jnp.concatenate([p, p], axis=0)) for x, p in zip(biased, peaks)
+    ]
+    totals = [jnp.sum(x, axis=1, keepdims=True) for x in weights]
+    values = [
+        jnp.dot(weights[r].astype(jnp.bfloat16), both(r), preferred_element_type=jnp.float32)
+        for r in range(rows)
+    ]
     lane = lax.broadcasted_iota(jnp.int32, (heads, width), 1)
+    tiles = []
     for r in range(rows):
-        both = jnp.concatenate([cache_ref[r, :half], cache_ref[r, half:]], axis=1)
-        scores = lax.dot_general(
-            query_ref[r], both, (((1,), (1,)), ((), ())), preferred_element_type=jnp.float32
-        )
-        biased = scores * scale - bias_ref[r]
-        peak = jnp.max(biased, axis=1, keepdims=True)
-        peak = jnp.maximum(jnp.maximum(peak[:heads], peak[heads:]), masked_floor)
-        weights = jnp.exp(biased - jnp.concatenate([peak, peak], axis=0))
-        total = jnp.sum(weights, axis=1, keepdims=True)
-        total = total[:heads] + total[heads:]
-        values = jnp.dot(weights.astype(jnp.bfloat16), both, preferred_element_type=jnp.float32)
-        values = values[:heads, :width] + values[heads:, width:]
-        out_ref[r] = jnp.where(lane == 0, peak, jnp.where(lane == 1, total, values))
-
-
-def attend(query, cache, bias, scale):
+        tile = values[r][:heads, :width] + values[r][heads:, width:]
+        total = totals[r][:heads] + totals[r][heads:]
+        tile = jnp.where(lane == 0, peaks[r], jnp.where(lane == 1, total, tile))
+        tiles.append(jnp.where(lane == 2, last_ref[r], tile))
+    by_head = jnp.swapaxes(jnp.stack(tiles), 0, 1)
+    lane = lax.broadcasted_iota(jnp.int32, (rows, width), 1)
+    fields = [jnp.zeros((rows, width), jnp.float32) for _ in range(3)]
+    for h in range(heads):
+        tile = by_head[h]
+        for f in range(3):
+            fields[f] = jnp.where(lane == h, tile[:, f : f + 1], fields[f])
+        if h % 2:
+            pair = jnp.where(lane < size, pltpu.roll(by_head[h - 1], size, 1), tile)
+            out_ref[:, (h - 1) * size : (h + 1) * size] = pair.astype(out_ref.dtype)
+    stats = sum(write_field(fields[f], f, heads) for f in range(3))
+    out_ref[:, heads * size :] = stats.astype(out_ref.dtype)
+
+
+def attend(query, cache, bias, last, scale):
     batch, length, width = cache.shape
-    rows = 4
+    rows = 8
     heads = query.shape[1] // 2
 
     def spec(*shape):
         return pl.BlockSpec((rows,) + shape, lambda i: (i, 0, 0))
 
+    full = heads * width // 2 + lanes
     return pl.pallas_call(
         functools.partial(attend_body, scale=scale),
         grid=(batch // rows,),
@@ -131,11 +159,53 @@
             spec(2 * heads, 2 * width),
             spec(length, width),
             spec(2 * heads, length // 2),
+            spec(heads, lanes),
         ],
-        out_specs=spec(heads, width),
-        out_shape=jax.ShapeDtypeStruct((batch, heads, width), jnp.float32),
+        out_specs=pl.BlockSpec((rows, full), lambda i: (i, 0)),
+        out_shape=jax.ShapeDtypeStruct((batch, full), jnp.bfloat16),
         name="attend",
-    )(query, cache, bias)
+    )(query, cache, bias, last)
+
+
+def project_body(at_ref, tokens_ref, gain_ref, query_ref, key_ref, value_ref, gate_ref, out_ref):
+    x = tokens_ref[...].astype(jnp.float32)
+    squares = jnp.sum(x * x, axis=1, keepdims=True)
+    normed = (x * gain_ref[...]).astype(jnp.bfloat16)
+    start = 0
+    for ref in (query_ref, key_ref, value_ref):
+        part = jnp.dot(normed, ref[...], preferred_element_type=jnp.float32)
+        out_ref[:, start : start + part.shape[1]] = part.astype(out_ref.dtype)
+        start += part.shape[1]
+    gate = lax.dot_general(
+        normed, gate_ref[...], (((1,), (1,)), ((), ())), preferred_element_type=jnp.float32
+    )
+    rest = out_ref.shape[1] - start
+    tail = jnp.concatenate(
+        [gate, jnp.broadcast_to(squares, (x.shape[0], rest - gate.shape[1]))], axis=1
+    )
+    out_ref[:, start:] = tail.astype(out_ref.dtype)
+
+
+def project(at, tokens, gain, w_query, w_key, w_value, gates):
+    batch, cols = tokens.shape
+    used = w_query.shape[1] + w_key.shape[1] + w_value.shape[1] + gates.shape[0] + 1
+    total = used + -used % lanes
+
+    def whole(x):
+        return pl.BlockSpec(x.shape, lambda i, at: (0, 0))
+
+    return pl.pallas_call(
+        project_body,
+        grid_spec=pltpu.PrefetchScalarGridSpec(
+            num_scalar_prefetch=1,
+            grid=(1,),
+            in_specs=[whole(x) for x in (tokens, gain, w_query, w_key, w_value)]
+            + [pl.BlockSpec((gates.shape[0], cols), lambda i, at: (0, at[0]))],
+            out_specs=pl.BlockSpec((batch, total), lambda i, at: (0, 0)),
+        ),
+        out_shape=jax.ShapeDtypeStruct((batch, total), jnp.bfloat16),
+        name="project",
+    )(at, tokens, gain, w_query, w_key, w_value, gates)
 
 
 def read_field(stats, index, heads):
@@ -211,6 +281,8 @@
 def merge(mine, other, heads, head_size):
     return pl.pallas_call(
         functools.partial(merge_body, heads=heads, head_size=head_size),
+        in_specs=[pl.BlockSpec(memory_space=pltpu.VMEM)] * 2,
+        out_specs=pl.BlockSpec(memory_space=pltpu.VMEM),
         out_shape=jax.ShapeDtypeStruct(mine.shape, mine.dtype),
         name="merge",
     )(mine, other)
@@ -247,19 +319,14 @@
     batch = mine.shape[0]
     return pl.pallas_call(
         functools.partial(finish_body, heads=heads, head_size=head_size),
+        in_specs=[pl.BlockSpec(memory_space=pltpu.VMEM)] * 4,
+        out_specs=[pl.BlockSpec(memory_space=pltpu.VMEM)] * 2,
         out_shape=[
             jax.ShapeDtypeStruct((batch, heads * head_size), jnp.bfloat16),
             jax.ShapeDtypeStruct((batch, lanes), jnp.float32),
         ],
         name="finish",
     )(mine, other, fresh, value)
-
-
-def split_three(x):
-    high = lax.reduce_precision(x, 8, 7)
-    mid = lax.reduce_precision(x - high, 8, 7)
-    low = lax.reduce_precision(x - high - mid, 8, 7)
-    return [high, mid, low]
 
 
 def shards(
@@ -288,28 +355,25 @@
     first_pos = lax.axis_index("kv") * span
     bias, last_cum = expand_gates(lengths - first_pos, cum_gates, kv_local, group)
 
-    tokens_f = tokens.astype(jnp.float32)
-    squares = jnp.sum(tokens_f * tokens_f, axis=1, keepdims=True)
-    normed = (tokens_f * norm_gain).astype(jnp.bfloat16)
-    gate_cols = lax.dynamic_slice(
-        forget_weight,
-        (lax.axis_index("kv") * cols, lax.axis_index("tp") * heads),
-        (cols, heads),
-    )
-    parts = [
-        jnp.dot(normed, w, preferred_element_type=jnp.float32)
-        for w in (w_query, w_key, w_value, gate_cols)
-    ]
-    parts.append(squares)
-    used = sum(p.shape[1] for p in parts)
-    parts.append(jnp.zeros((batch, -used % lanes), jnp.float32))
-    sums = exchange_sum(jnp.concatenate(parts, axis=1), "kv")
+    parts = project(
+        lax.axis_index("kv").reshape(1),
+        tokens,
+        norm_gain.reshape(1, cols),
+        w_query,
+        w_key,
+        w_value,
+        forget_weight.T,
+    )
+    sums = exchange_sum(parts, "kv")
 
     edge = width + 2 * kv_width
-    row_scale = lax.rsqrt(sums[:, edge + heads : edge + heads + 1] / model_width + norm_eps)
+    all_heads = forget_weight.shape[1]
+    squares = sums[:, edge + all_heads : edge + all_heads + 1]
+    row_scale = lax.rsqrt(squares / model_width + norm_eps)
     projected = (row_scale * sums[:, :edge]).astype(jnp.bfloat16)
     query = projected[:, :width]
-    log_gate = jax.nn.log_sigmoid(row_scale * sums[:, edge : edge + heads] + forget_bias)
+    gates = lax.dynamic_slice(sums, (0, edge + lax.axis_index("tp") * heads), (batch, heads))
+    log_gate = jax.nn.log_sigmoid(row_scale * gates + forget_bias)
     query_rows = query.reshape(batch, heads, head_size)
     full = 4 * head_size
     query_pair = jnp.concatenate(
@@ -321,7 +385,7 @@
     )
     scale = head_size ** (-0.5)
     cache = kv_cache.reshape(batch, span * kv_local, 2 * head_size)
-    partial = attend(query_pair, cache, bias, scale)
+    packed = attend(query_pair, cache, bias, last_cum, scale)
 
     key_rows = projected[:, width : width + kv_width].reshape(batch, kv_local, 1, head_size)
     fresh_score = jnp.sum(
@@ -342,13 +406,6 @@
         batch, width
     )
 
-    stats = split_three(partial[:, :, 0]) + split_three(partial[:, :, 1])
-    stats = stats + split_three(last_cum[:, :, 0])
-    stats.append(jnp.zeros((batch, lanes - 9 * heads), jnp.float32))
-    packed = jnp.concatenate(
-        [partial[:, :, head_size:].reshape(batch, width)] + stats, axis=1
-    ).astype(jnp.bfloat16)
-
     step = 1
     while 2 * step < lax.axis_size("kv"):
         packed = merge(packed, xor_permute(packed, "kv", step), heads, head_size)

time: 81.5 us -> 65.1 us (0.80)
  Pallas kernels: 31.8 us -> 25.5 us
  local copies, waits for them, and re-layouts: 10.5 us -> 4.61 us
  matrix products: 4.96 us -> 0.94 us
  waiting for transfers between devices: 13.8 us -> 15.3 us
  starting transfers between devices: 14.1 us -> 12.9 us
    pallas_call x1, Pallas kernels: 21.5 us -> 13.1 us  [attend(): pl.pallas_call(functools.partial(attend_body, scale=scale), grid=(batch /...]
    dot_general x4 -> x0, matrix products: 4.02 us -> none  [shards(): jnp.dot(normed, w, preferred_element_type=jnp.float32)]
    pallas_call x1 -> x0, local copies, waits for them, and re-layouts: 2.74 us -> none  [expand_gates(): pl.pallas_call(functools.partial(expand_body, kv_local=kv_local, group=gr...]
    slice x2 -> x0, local copies, waits for them, and re-layouts: 2.11 us -> none  [the longest x1 1.07 us: shards(): stats = split_three(partial[:, :, 0]) + split_three(partial[:, :, 1])]
    pallas_call x0 -> x1, Pallas kernels: none -> 2.09 us  [project(): pl.pallas_call(project_body, grid_spec=pltpu.PrefetchScalarGridSpec(num_s...]
    ppermute x8, waiting for transfers between devices: 13.8 us -> 15.3 us  [xor_permute(): return lax.ppermute(x, axis, [(i, i ^ step) for i in range(size)])]
    ppermute x8, starting transfers between devices: 14.1 us -> 12.9 us  [xor_permute(): return lax.ppermute(x, axis, [(i, i ^ step) for i in range(size)])]
    reduce_sum x1 -> x0, other arithmetic: 0.93 us -> none  [shards(): squares = jnp.sum(tokens_f * tokens_f, axis=1, keepdims=True)]
  transfers between devices with their start and end apart: 8 -> 8, of which waited for: 7 -> 7; matrix products, arithmetic and copies ran while one was open for 9% -> 7% of each run, Pallas kernels for 7% -> 8%
where the time goes in v2:
time: 65.1 us; the launch traced here: 64.5 us
  Pallas kernels  25.5 us (39%)
  waiting for transfers between devices  15.3 us (24%)
  starting transfers between devices  12.9 us (20%)
  other arithmetic  4.63 us (7%)
  local copies, waits for them, and re-layouts  4.61 us (7%)
  matrix products  0.94 us (1%)
  between operations  0.74 us (1%)
    ppermute x8, waiting for transfers between devices, xor_permute(): return lax.ppermute(x, axis, [(i, i ^ step) for i in range(size)])  15.3 us
    pallas_call x1, Pallas kernels, attend(): pl.pallas_call(functools.partial(attend_body, scale=scale), grid=(batch /...  13.1 us
    ppermute x8, starting transfers between devices, xor_permute(): return lax.ppermute(x, axis, [(i, i ^ step) for i in range(size)])  12.9 us
    pallas_call x1, Pallas kernels, expand_gates(): pl.pallas_call(functools.partial(expand_body, kv_local=kv_local, group=gr...  5.32 us
    pallas_call x2, Pallas kernels, merge(): pl.pallas_call(functools.partial(merge_body, heads=heads, head_size=head_...  3.28 us
    unnamed x11, local copies, waits for them, and re-layouts  3.22 us
    pallas_call x1, Pallas kernels, project(): pl.pallas_call(project_body, grid_spec=pltpu.PrefetchScalarGridSpec(num_s...  2.09 us
    pallas_call x1, Pallas kernels, finish(): pl.pallas_call(functools.partial(finish_body, heads=heads, head_size=head...  1.69 us
  transfers between devices with their start and end apart: 8, of which 7 were waited for; matrix products, arithmetic and copies ran while one was open for 7% of the time, Pallas kernels for 8%

profile of v2, /device:TPU:0, one launch (start us, length us, event | category | flops | bytes accessed | tf_op | source)
XLA Modules:
  0.0 64.5 jit_solution(17437637174899443463)
XLA Ops:
  0.6 0.0 copy-start
  0.7 2.1 %project.1 = bf16[32,896]{1,0:T(8,128)(2,1)} custom-call(s32[1]{0:T(128)} %bitcast.at_ref, bf16[32,512]{1,0:T(8,128)(2,1)} %tokens_ref.1, f32[1,512]{1,0:T(1,128)} %bitcast.12, bf16[512,512]{1,0:T(8,128)(2,1)} %query_ref.1, bf16[512,128]{1,0:T(8,128)(2,1)} %key_ref.1, bf16[512,128]{1,0:T(8,128)(2,1)} %value_ref.1, bf16[32,4096]{1,0:T(8,128)(2,1)} %bitcast.9), custom_call_target="tpu_custom_call" | custom-call | tf_op jit(solution)/shard_map/project/pallas_call | solution.py:197
  2.7 3.0 %collective-permute-start = (bf16[32,896]{1,0:T(8,128)(2,1)}, bf16[32,896]{1,0:T(8,128)(2,1)S(1)}, u32[]{:S(2)}, u32[]{:S(2)}) collective-permute-start(bf16[32,896]{1,0:T(8,128)(2,1)} %project.1), channel_id=1, source_target_pairs={{0,4},{4,0},{8,12},{12,8},{16,20},{20,16},{24,28},{28,24},{1,5},{5... | collective-permute-start | bytes 172040 | tf_op jit(solution)/shard_map/ppermute | solution.py:21
  5.7 2.4 %collective-permute-done = bf16[32,896]{1,0:T(8,128)(2,1)S(1)} collective-permute-done((bf16[32,896]{1,0:T(8,128)(2,1)}, bf16[32,896]{1,0:T(8,128)(2,1)S(1)}, u32[]{:S(2)}, u32[]{:S(2)}) %collective-permute-start) | collective-permute-done | bytes 57376 | tf_op jit(solution)/shard_map/ppermute | solution.py:21
  8.1 0.8 %add_convert_fusion.1 = bf16[32,896]{1,0:T(8,128)(2,1)S(1)} fusion(bf16[32,896]{1,0:T(8,128)(2,1)S(1)} %collective-permute-done, bf16[32,896]{1,0:T(8,128)(2,1)} %project.1), kind=kLoop, calls=%fused_computation.9 | loop fusion | flops 114688 | bytes 172032 | tf_op jit(solution)/shard_map/convert_element_type | solution.py:27
  8.9 2.1 %collective-permute-start.1 = (bf16[32,896]{1,0:T(8,128)(2,1)S(1)}, bf16[32,896]{1,0:T(8,128)(2,1)S(1)}, u32[]{:S(2)}, u32[]{:S(2)}) collective-permute-start(bf16[32,896]{1,0:T(8,128)(2,1)S(1)} %add_convert_fusion.1), channel_id=1, source_target_pairs={{0,8},{4,12},{8,0},{12,4},{16,24},{20,28},{24,16},{28,20},{1,9},{5... | collective-permute-start | bytes 172040 | tf_op jit(solution)/shard_map/ppermute | solution.py:21
  11.1 2.2 %collective-permute-done.1 = bf16[32,896]{1,0:T(8,128)(2,1)S(1)} collective-permute-done((bf16[32,896]{1,0:T(8,128)(2,1)S(1)}, bf16[32,896]{1,0:T(8,128)(2,1)S(1)}, u32[]{:S(2)}, u32[]{:S(2)}) %collective-permute-start.1) | collective-permute-done | bytes 57376 | tf_op jit(solution)/shard_map/ppermute | solution.py:21
  13.3 3.1 %collective-permute-start.2 = (bf16[32,896]{1,0:T(8,128)(2,1)S(1)}, bf16[32,896]{1,0:T(8,128)(2,1)S(1)}, u32[]{:S(2)}, u32[]{:S(2)}) collective-permute-start(bf16[32,896]{1,0:T(8,128)(2,1)S(1)} %add_convert_fusion), channel_id=1, source_target_pairs={{0,16},{4,20},{8,24},{12,28},{16,0},{20,4},{24,8},{28,12},{1,17},{... | collective-permute-start | bytes 172040 | tf_op jit(solution)/shard_map/ppermute | solution.py:21
  16.4 1.2 %broadcast_subtract_fusion.rel_ref = s32[32]{0:T(128)} fusion(s32[32]{0:T(128)} %param.20, s32[]{:T(128)S(6)} %mul.44), kind=kLoop, calls=%fused_computation.23 | loop fusion | flops 32 | bytes 260 | tf_op jit(solution)/shard_map/sub | solution.py:356
  17.5 0.1 pad.12.clone
  17.6 5.3 %expand_gates.1 = (f32[32,16,1280]{2,1,0:T(8,128)}, f32[32,8,128]{2,1,0:T(8,128)}) custom-call(s32[32]{0:T(128)} %broadcast_subtract_fusion.rel_ref, f32[32,8,1280]{2,1,0:T(8,128)} %cum_ref.1), custom_call_target="tpu_custom_call" | custom-call | tf_op jit(solution)/shard_map/expand_gates/pallas_call | solution.py:79
  22.9 0.0 collective-permute-done.2
  23.0 0.2 fusion.7
  23.1 0.1 fusion.3
  23.3 0.1 reshape.44
  23.3 0.1 reshape.43
  23.5 0.1 reshape.40
  23.6 0.7 %fusion.2.query_ref = bf16[32,16,256]{2,1,0:T(8,128)(2,1)} fusion(bf16[32,8,64]{2,1,0:T(8,128)(2,1)S(1)} %reshape.40), kind=kLoop, calls=%fused_computation.5 | loop fusion | flops 1048576 | bytes 294912 | tf_op jit(solution)/shard_map/concatenate | solution.py:379
  24.3 0.0 copy-start.4
  24.3 13.1 %attend.1.mine_ref = bf16[32,640]{1,0:T(8,128)(2,1)} custom-call(bf16[32,16,256]{2,1,0:T(8,128)(2,1)} %fusion.2.query_ref, bf16[32,2560,128]{2,1,0:T(8,128)(2,1)} %bitcast.8, f32[32,16,1280]{2,1,0:T(8,128)} %get-tuple-element.6.bias_ref, f32[32,8,128]{2,1,0:T(8,128)} %get-tuple-element.7.last_ref), custom_call_target="tpu_custom_call" | custom-call | tf_op jit(solution)/shard_map/attend/pallas_call | solution.py:155
  37.4 1.5 %collective-permute-start.3 = (bf16[32,640]{1,0:T(8,128)(2,1)}, bf16[32,640]{1,0:T(8,128)(2,1)S(1)}, u32[]{:S(2)}, u32[]{:S(2)}) collective-permute-start(bf16[32,640]{1,0:T(8,128)(2,1)} %attend.1.mine_ref), channel_id=1, source_target_pairs={{0,4},{4,0},{8,12},{12,8},{16,20},{20,16},{24,28},{28,24},{1,5},{5... | collective-permute-start | bytes 122888 | tf_op jit(solution)/shard_map/ppermute | solution.py:21
  38.9 0.0 copy-done.4
  38.9 0.1 fusion.4
  39.0 0.2 multiply_reduce_fusion
  39.2 0.1 copy.19
  39.3 2.3 %collective-permute-done.3.other_ref = bf16[32,640]{1,0:T(8,128)(2,1)S(1)} collective-permute-done((bf16[32,640]{1,0:T(8,128)(2,1)}, bf16[32,640]{1,0:T(8,128)(2,1)S(1)}, u32[]{:S(2)}, u32[]{:S(2)}) %collective-permute-start.3) | collective-permute-done | bytes 40992 | tf_op jit(solution)/shard_map/ppermute | solution.py:21
  41.6 0.6 copy-done.2
  42.2 1.6 %merge.2.mine_ref = bf16[32,640]{1,0:T(8,128)(2,1)} custom-call(bf16[32,640]{1,0:T(8,128)(2,1)} %attend.1.mine_ref, bf16[32,640]{1,0:T(8,128)(2,1)} %copy-done.2), custom_call_target="tpu_custom_call" | custom-call | tf_op jit(solution)/shard_map/merge/pallas_call | solution.py:282
  43.9 1.6 %collective-permute-start.4 = (bf16[32,640]{1,0:T(8,128)(2,1)}, bf16[32,640]{1,0:T(8,128)(2,1)S(1)}, u32[]{:S(2)}, u32[]{:S(2)}) collective-permute-start(bf16[32,640]{1,0:T(8,128)(2,1)} %merge.2.mine_ref), channel_id=1, source_target_pairs={{0,8},{4,12},{8,0},{12,4},{16,24},{20,28},{24,16},{28,20},{1,9},{5... | collective-permute-start | bytes 122888 | tf_op jit(solution)/shard_map/ppermute | solution.py:21
  45.5 0.1 copy.20
  45.5 2.6 %collective-permute-done.4.other_ref = bf16[32,640]{1,0:T(8,128)(2,1)S(1)} collective-permute-done((bf16[32,640]{1,0:T(8,128)(2,1)}, bf16[32,640]{1,0:T(8,128)(2,1)S(1)}, u32[]{:S(2)}, u32[]{:S(2)}) %collective-permute-start.4) | collective-permute-done | bytes 40992 | tf_op jit(solution)/shard_map/ppermute | solution.py:21
  48.1 0.6 copy-done.3
  48.7 1.6 %merge.3.mine_ref = bf16[32,640]{1,0:T(8,128)(2,1)} custom-call(bf16[32,640]{1,0:T(8,128)(2,1)} %merge.2.mine_ref, bf16[32,640]{1,0:T(8,128)(2,1)} %copy-done.3), custom_call_target="tpu_custom_call" | custom-call | tf_op jit(solution)/shard_map/merge/pallas_call | solution.py:282
  50.3 0.0 collective-permute-start.5
  50.3 0.7 %maximum_maximum_fusion.fresh_ref = f32[32,128]{1,0:T(8,128)} fusion(f32[32,8]{1,0:T(8,128)S(1)} %fusion.4, f32[32,8]{1,0:T(8,128)S(1)} %copy.20, f32[128]{0:T(128)S(1)} %pad.12.clone), kind=kLoop, calls=%fused_computation.20 | loop fusion | flops 8192 | bytes 18944 | tf_op jit(solution)/shard_map/concatenate | solution.py:396
  51.0 0.1 broadcast_in_dim.12
  51.1 0.7 %reshape.42.value_ref = bf16[32,512]{1,0:T(8,128)(2,1)} reshape(bf16[32,2,4,64]{3,2,1,0:T(4,128)(2,1)S(1)} %broadcast_in_dim.13) | data formatting | bytes 65536 | tf_op jit(solution)/shard_map/reshape | solution.py:405
  51.9 3.6 %collective-permute-done.5.other_ref = bf16[32,640]{1,0:T(8,128)(2,1)S(1)} collective-permute-done((bf16[32,640]{1,0:T(8,128)(2,1)}, bf16[32,640]{1,0:T(8,128)(2,1)S(1)}, u32[]{:S(2)}, u32[]{:S(2)}) %collective-permute-start.5) | collective-permute-done | bytes 40992 | tf_op jit(solution)/shard_map/ppermute | solution.py:21
  55.5 0.6 copy-done.1
  56.1 1.7 %finish.1 = (bf16[32,512]{1,0:T(8,128)(2,1)}, f32[32,128]{1,0:T(8,128)}) custom-call(bf16[32,640]{1,0:T(8,128)(2,1)} %merge.3.mine_ref, bf16[32,640]{1,0:T(8,128)(2,1)} %copy-done.1, f32[32,128]{1,0:T(8,128)} %maximum_maximum_fusion.fresh_ref, bf16[32,512]{1,0:T(8,128)(2,1)} %reshape.42.value_ref), custom_call_target="tpu_custom_call" | custom-call | tf_op jit(solution)/shard_map/finish/pallas_call | solution.py:320
  57.8 0.0 copy-done
  57.8 0.9 %convolution_convert_fusion = bf16[32,512]{1,0:T(8,128)(2,1)S(1)} fusion(bf16[32,512]{1,0:T(8,128)(2,1)} %get-tuple-element.8, bf16[512,512]{1,0:T(8,128)(2,1)S(1)} %copy-done), kind=kOutput, calls=%fused_computation | convolution fusion | flops 16793600 | bytes 589824 | tf_op jit(solution)/shard_map/dot_general | solution.py:416
  58.7 0.0 collective-permute-start.6
  58.7 1.2 %collective-permute-done.6 = bf16[32,512]{1,0:T(8,128)(2,1)S(1)} collective-permute-done((bf16[32,512]{1,0:T(8,128)(2,1)S(1)}, bf16[32,512]{1,0:T(8,128)(2,1)S(1)}, u32[]{:S(2)}, u32[]{:S(2)}) %collective-permute-start.6) | collective-permute-done | bytes 32800 | tf_op jit(solution)/shard_map/ppermute | solution.py:21
  59.9 1.5 %collective-permute-start.7 = (bf16[32,512]{1,0:T(8,128)(2,1)S(1)}, bf16[32,512]{1,0:T(8,128)(2,1)S(1)}, u32[]{:S(2)}, u32[]{:S(2)}) collective-permute-start(bf16[32,512]{1,0:T(8,128)(2,1)S(1)} %add_convert_fusion.3), channel_id=1, source_target_pairs={{0,2},{1,3},{2,0},{3,1},{4,6},{5,7},{6,4},{7,5},{8,10},{9,11},{10,... | collective-permute-start | bytes 98312 | tf_op jit(solution)/shard_map/ppermute | solution.py:21
  61.5 1.4 %copy.21 = f32[32,8]{0,1:T(8,128)} copy(f32[32,8]{1,0:T(8,128)} %bitcast.10) | data formatting | bytes 2048
  62.9 1.1 %collective-permute-done.7 = bf16[32,512]{1,0:T(8,128)(2,1)S(1)} collective-permute-done((bf16[32,512]{1,0:T(8,128)(2,1)S(1)}, bf16[32,512]{1,0:T(8,128)(2,1)S(1)}, u32[]{:S(2)}, u32[]{:S(2)}) %collective-permute-start.7) | collective-permute-done | bytes 32800 | tf_op jit(solution)/shard_map/ppermute | solution.py:21
  63.9 0.6 add_convert_fusion.2
  (11 shorter events, 0.1 us)
Async XLA Ops:
  0.6 57.1 %copy-start = (bf16[512,512]{1,0:T(8,128)(2,1)S(1)}, bf16[512,512]{1,0:T(8,128)(2,1)}, u32[]{:S(2)}) copy-start(bf16[512,512]{1,0:T(8,128)(2,1)} %param.21) | copy-start | bytes 1572868
  2.7 5.4 %collective-permute-start = (bf16[32,896]{1,0:T(8,128)(2,1)}, bf16[32,896]{1,0:T(8,128)(2,1)S(1)}, u32[]{:S(2)}, u32[]{:S(2)}) collective-permute-start(bf16[32,896]{1,0:T(8,128)(2,1)} %project.1), channel_id=1, source_target_pairs={{0,4},{4,0},{8,12},{12,8},{16,20},{20,16},{24,28},{28,24},{1,5},{5... | collective-permute-start | bytes 172040 | tf_op jit(solution)/shard_map/ppermute | solution.py:21
  8.9 4.3 %collective-permute-start.1 = (bf16[32,896]{1,0:T(8,128)(2,1)S(1)}, bf16[32,896]{1,0:T(8,128)(2,1)S(1)}, u32[]{:S(2)}, u32[]{:S(2)}) collective-permute-start(bf16[32,896]{1,0:T(8,128)(2,1)S(1)} %add_convert_fusion.1), channel_id=1, source_target_pairs={{0,8},{4,12},{8,0},{12,4},{16,24},{20,28},{24,16},{28,20},{1,9},{5... | collective-permute-start | bytes 172040 | tf_op jit(solution)/shard_map/ppermute | solution.py:21
  13.3 9.7 %collective-permute-start.2 = (bf16[32,896]{1,0:T(8,128)(2,1)S(1)}, bf16[32,896]{1,0:T(8,128)(2,1)S(1)}, u32[]{:S(2)}, u32[]{:S(2)}) collective-permute-start(bf16[32,896]{1,0:T(8,128)(2,1)S(1)} %add_convert_fusion), channel_id=1, source_target_pairs={{0,16},{4,20},{8,24},{12,28},{16,0},{20,4},{24,8},{28,12},{1,17},{... | collective-permute-start | bytes 172040 | tf_op jit(solution)/shard_map/ppermute | solution.py:21
  24.3 14.6 %copy-start.4 = (f32[8]{0:T(128)S(1)}, f32[8]{0:T(128)}, u32[]{:S(2)}) copy-start(f32[8]{0:T(128)} %param.17) | copy-start | bytes 100
  37.4 4.2 %collective-permute-start.3 = (bf16[32,640]{1,0:T(8,128)(2,1)}, bf16[32,640]{1,0:T(8,128)(2,1)S(1)}, u32[]{:S(2)}, u32[]{:S(2)}) collective-permute-start(bf16[32,640]{1,0:T(8,128)(2,1)} %attend.1.mine_ref), channel_id=1, source_target_pairs={{0,4},{4,0},{8,12},{12,8},{16,20},{20,16},{24,28},{28,24},{1,5},{5... | collective-permute-start | bytes 122888 | tf_op jit(solution)/shard_map/ppermute | solution.py:21
  41.6 0.6 copy-start.2
  43.9 4.2 %collective-permute-start.4 = (bf16[32,640]{1,0:T(8,128)(2,1)}, bf16[32,640]{1,0:T(8,128)(2,1)S(1)}, u32[]{:S(2)}, u32[]{:S(2)}) collective-permute-start(bf16[32,640]{1,0:T(8,128)(2,1)} %merge.2.mine_ref), channel_id=1, source_target_pairs={{0,8},{4,12},{8,0},{12,4},{16,24},{20,28},{24,16},{28,20},{1,9},{5... | collective-permute-start | bytes 122888 | tf_op jit(solution)/shard_map/ppermute | solution.py:21
  48.1 0.6 copy-start.3
  50.3 5.1 %collective-permute-start.5 = (bf16[32,640]{1,0:T(8,128)(2,1)}, bf16[32,640]{1,0:T(8,128)(2,1)S(1)}, u32[]{:S(2)}, u32[]{:S(2)}) collective-permute-start(bf16[32,640]{1,0:T(8,128)(2,1)} %merge.3.mine_ref), channel_id=1, source_target_pairs={{0,16},{4,20},{8,24},{12,28},{16,0},{20,4},{24,8},{28,12},{1,17},{... | collective-permute-start | bytes 122888 | tf_op jit(solution)/shard_map/ppermute | solution.py:21
  55.5 0.6 copy-start.1
  58.7 1.2 %collective-permute-start.6 = (bf16[32,512]{1,0:T(8,128)(2,1)S(1)}, bf16[32,512]{1,0:T(8,128)(2,1)S(1)}, u32[]{:S(2)}, u32[]{:S(2)}) collective-permute-start(bf16[32,512]{1,0:T(8,128)(2,1)S(1)} %convolution_convert_fusion), channel_id=1, source_target_pairs={{0,1},{1,0},{2,3},{3,2},{4,5},{5,4},{6,7},{7,6},{8,9},{9,8},{10,11... | collective-permute-start | bytes 98312 | tf_op jit(solution)/shard_map/ppermute | solution.py:21
  59.9 4.0 %collective-permute-start.7 = (bf16[32,512]{1,0:T(8,128)(2,1)S(1)}, bf16[32,512]{1,0:T(8,128)(2,1)S(1)}, u32[]{:S(2)}, u32[]{:S(2)}) collective-permute-start(bf16[32,512]{1,0:T(8,128)(2,1)S(1)} %add_convert_fusion.3), channel_id=1, source_target_pairs={{0,2},{1,3},{2,0},{3,1},{4,6},{5,7},{6,4},{7,5},{8,10},{9,11},{10,... | collective-permute-start | bytes 98312 | tf_op jit(solution)/shard_map/ppermute | solution.py:21

commit v3 on v2

--- a/solution.py
+++ b/solution.py
@@ -10,6 +10,10 @@
 norm_eps = 1e-05
 masked_floor = -1e30
 lanes = 128
+
+
+def in_vmem(x):
+    return pltpu.with_memory_space_constraint(x, pltpu.VMEM)
 
 
 def rounded(x):
@@ -31,7 +35,7 @@
     return x
 
 
-def expand_body(rel_ref, cum_ref, bias_ref, last_ref, *, kv_local, group):
+def expand_body(lengths_ref, first_ref, cum_ref, bias_ref, last_ref, *, kv_local, group):
     rows, heads, span = cum_ref.shape
     wide = lanes * kv_local
     half = span * kv_local // 2
@@ -46,7 +50,9 @@
     local = col // kv_local
     narrow = lax.broadcasted_iota(jnp.int32, (heads, lanes), 1)
     base = pl.program_id(0) * rows
+    rels = [lengths_ref[base + r] - first_ref[0] for r in range(rows)]
     last = [jnp.zeros((heads, lanes), jnp.float32) for _ in range(rows)]
+    spread_rows = []
     for c in range(span // lanes):
         x = cum_ref[:, :, c * lanes : (c + 1) * lanes].reshape(rows * heads, lanes)
         high = rounded(x)
@@ -56,35 +62,37 @@
         y = jnp.dot(pair, spread2, preferred_element_type=jnp.float32) + jnp.dot(
             low, spread, preferred_element_type=jnp.float32
         )
+        spread_rows.append(y)
+        for r in range(rows):
+            last[r] = last[r] + jnp.where(
+                narrow == rels[r] - 1 - c * lanes, x[r * heads : (r + 1) * heads], 0.0
+            )
+    for c in range(span // lanes):
         start = c * wide
         side = start // half
         start = start - side * half
         for r in range(rows):
-            rel = rel_ref[base + r] - c * lanes
-            ok = own & (local < rel)
+            ok = own & (local < rels[r] - c * lanes)
             bias_ref[r, side * heads : (side + 1) * heads, start : start + wide] = jnp.where(
-                ok, y[r * heads : (r + 1) * heads], -masked_floor
-            )
-            last[r] = last[r] + jnp.where(
-                narrow == rel - 1, x[r * heads : (r + 1) * heads], 0.0
+                ok, spread_rows[c][r * heads : (r + 1) * heads], -masked_floor
             )
     for r in range(rows):
         last_ref[r] = jnp.broadcast_to(jnp.sum(last[r], axis=1, keepdims=True), (heads, lanes))
 
 
-def expand_gates(rel_len, cum_gates, kv_local, group):
+def expand_gates(lengths, first_pos, cum_gates, kv_local, group):
     batch, heads, span = cum_gates.shape
     rows = 8
     half = span * kv_local // 2
     return pl.pallas_call(
         functools.partial(expand_body, kv_local=kv_local, group=group),
         grid_spec=pltpu.PrefetchScalarGridSpec(
-            num_scalar_prefetch=1,
+            num_scalar_prefetch=2,
             grid=(batch // rows,),
-            in_specs=[pl.BlockSpec((rows, heads, span), lambda i, rel: (i, 0, 0))],
+            in_specs=[pl.BlockSpec((rows, heads, span), lambda i, n, f: (i, 0, 0))],
             out_specs=[
-                pl.BlockSpec((rows, 2 * heads, half), lambda i, rel: (i, 0, 0)),
-                pl.BlockSpec((rows, heads, lanes), lambda i, rel: (i, 0, 0)),
+                pl.BlockSpec((rows, 2 * heads, half), lambda i, n, f: (i, 0, 0)),
+                pl.BlockSpec((rows, heads, lanes), lambda i, n, f: (i, 0, 0)),
             ],
         ),
         out_shape=[
@@ -92,7 +100,7 @@
             jax.ShapeDtypeStruct((batch, heads, lanes), jnp.float32),
         ],
         name="expand_gates",
-    )(rel_len, cum_gates)
+    )(lengths, first_pos, cum_gates)
 
 
 def attend_body(query_ref, cache_ref, bias_ref, last_ref, out_ref, *, scale):
@@ -162,9 +170,9 @@
             spec(heads, lanes),
         ],
         out_specs=pl.BlockSpec((rows, full), lambda i: (i, 0)),
-        out_shape=jax.ShapeDtypeStruct((batch, full), jnp.bfloat16),
+        out_shape=pltpu.VMEM((batch, full), jnp.bfloat16),
         name="attend",
-    )(query, cache, bias, last)
+    )(in_vmem(query), cache, bias, last)
 
 
 def project_body(at_ref, tokens_ref, gain_ref, query_ref, key_ref, value_ref, gate_ref, out_ref):
@@ -203,7 +211,7 @@
             + [pl.BlockSpec((gates.shape[0], cols), lambda i, at: (0, at[0]))],
             out_specs=pl.BlockSpec((batch, total), lambda i, at: (0, 0)),
         ),
-        out_shape=jax.ShapeDtypeStruct((batch, total), jnp.bfloat16),
+        out_shape=pltpu.VMEM((batch, total), jnp.bfloat16),
         name="project",
     )(at, tokens, gain, w_query, w_key, w_value, gates)
 
@@ -283,9 +291,9 @@
         functools.partial(merge_body, heads=heads, head_size=head_size),
         in_specs=[pl.BlockSpec(memory_space=pltpu.VMEM)] * 2,
         out_specs=pl.BlockSpec(memory_space=pltpu.VMEM),
-        out_shape=jax.ShapeDtypeStruct(mine.shape, mine.dtype),
+        out_shape=pltpu.VMEM(mine.shape, mine.dtype),
         name="merge",
-    )(mine, other)
+    )(in_vmem(mine), in_vmem(other))
 
 
 def finish_body(
@@ -322,11 +330,11 @@
         in_specs=[pl.BlockSpec(memory_space=pltpu.VMEM)] * 4,
         out_specs=[pl.BlockSpec(memory_space=pltpu.VMEM)] * 2,
         out_shape=[
-            jax.ShapeDtypeStruct((batch, heads * head_size), jnp.bfloat16),
-            jax.ShapeDtypeStruct((batch, lanes), jnp.float32),
+            pltpu.VMEM((batch, heads * head_size), jnp.bfloat16),
+            pltpu.VMEM((batch, lanes), jnp.float32),
         ],
         name="finish",
-    )(mine, other, fresh, value)
+    )(in_vmem(mine), in_vmem(other), in_vmem(fresh), in_vmem(value))
 
 
 def shards(
@@ -353,7 +361,7 @@
     model_width = cols * lax.axis_size("kv")
 
     first_pos = lax.axis_index("kv") * span
-    bias, last_cum = expand_gates(lengths - first_pos, cum_gates, kv_local, group)
+    bias, last_cum = expand_gates(lengths, first_pos.reshape(1), cum_gates, kv_local, group)
 
     parts = project(
         lax.axis_index("kv").reshape(1),

time: 65.1 us -> 53.6 us (0.82)
  Pallas kernels: 25.5 us -> 20.1 us
  other arithmetic: 4.63 us -> 1.34 us
  local copies, waits for them, and re-layouts: 4.61 us -> 1.45 us
  waiting for transfers between devices: 15.3 us -> 16.4 us
  matrix products: 0.94 us -> 0.18 us
    pallas_call x2, Pallas kernels: 3.28 us -> 0.46 us  [merge(): pl.pallas_call(functools.partial(merge_body, heads=heads, head_size=head_...]
    unnamed x11 -> x5, local copies, waits for them, and re-layouts: 3.22 us -> 0.68 us
    pallas_call x1, Pallas kernels: 1.69 us -> 0.26 us  [finish(): pl.pallas_call(functools.partial(finish_body, heads=heads, head_size=head...]
    sub x1 -> x0, other arithmetic: 1.17 us -> none  [shards(): lengths - first_pos]
    ppermute x8, waiting for transfers between devices: 15.3 us -> 16.4 us  [xor_permute(): return lax.ppermute(x, axis, [(i, i ^ step) for i in range(size)])]
    convert_element_type x3, other arithmetic: 0.87 us -> 0.04 us  [exchange_sum(): mine = lax.optimization_barrier(x.astype(jnp.bfloat16))]
    dot_general x1, matrix products: 0.94 us -> 0.18 us  [shards(): part_out = jnp.dot(attended, w_out, preferred_element_type=jnp.float32)]
    concatenate x1, other arithmetic: 0.74 us -> 0.03 us  [shards(): jnp.concatenate([jnp.pad(query_rows, ((0, 0), (0, 0), (0, full - head_siz...]
  transfers between devices with their start and end apart: 8 -> 8, of which waited for: 7 -> 7; matrix products, arithmetic and copies ran while one was open for 7% -> 3% of each run, Pallas kernels for 8% -> 10%
where the time goes in v3:
time: 53.6 us; the launch traced here: 53.4 us
  Pallas kernels  20.1 us (38%)
  waiting for transfers between devices  16.4 us (31%)
  starting transfers between devices  13.1 us (24%)
  local copies, waits for them, and re-layouts  1.45 us (3%)
  other arithmetic  1.34 us (2%)
  between operations  0.78 us (1%)
    ppermute x8, waiting for transfers between devices, xor_permute(): return lax.ppermute(x, axis, [(i, i ^ step) for i in range(size)])  16.4 us
    ppermute x8, starting transfers between devices, xor_permute(): return lax.ppermute(x, axis, [(i, i ^ step) for i in range(size)])  13.1 us
    pallas_call x1, Pallas kernels, attend(): pl.pallas_call(functools.partial(attend_body, scale=scale), grid=(batch /...  12.6 us
    pallas_call x1, Pallas kernels, expand_gates(): pl.pallas_call(functools.partial(expand_body, kv_local=kv_local, group=gr...  5.32 us
    pallas_call x1, Pallas kernels, project(): pl.pallas_call(project_body, grid_spec=pltpu.PrefetchScalarGridSpec(num_s...  1.47 us
  transfers between devices with their start and end apart: 8, of which 7 were waited for; matrix products, arithmetic and copies ran while one was open for 3% of the time, Pallas kernels for 10%

profile of v3, /device:TPU:0, one launch (start us, length us, event | category | flops | bytes accessed | tf_op | source)
XLA Modules:
  0.0 53.4 jit_solution(16226613721095698801)
XLA Ops:
  0.6 0.0 copy-start
  0.7 1.5 %project.1 = bf16[32,896]{1,0:T(8,128)(2,1)S(1)} custom-call(s32[1]{0:T(128)} %bitcast.at_ref, bf16[32,512]{1,0:T(8,128)(2,1)} %tokens_ref.1, f32[1,512]{1,0:T(1,128)} %bitcast.13, bf16[512,512]{1,0:T(8,128)(2,1)} %query_ref.1, bf16[512,128]{1,0:T(8,128)(2,1)} %key_ref.1, bf16[512,128]{1,0:T(8,128)(2,1)} %value_ref.1, bf16[32,4096]{1,0:T(8,128)(2,1)} %bitcast.11), custom_call_target="tpu_custom_call" | custom-call | tf_op jit(solution)/shard_map/project/pallas_call | solution.py:205
  2.1 3.1 %collective-permute-start = (bf16[32,896]{1,0:T(8,128)(2,1)S(1)}, bf16[32,896]{1,0:T(8,128)(2,1)S(1)}, u32[]{:S(2)}, u32[]{:S(2)}) collective-permute-start(bf16[32,896]{1,0:T(8,128)(2,1)S(1)} %project.1), channel_id=1, source_target_pairs={{0,4},{4,0},{8,12},{12,8},{16,20},{20,16},{24,28},{28,24},{1,5},{5... | collective-permute-start | bytes 172040 | tf_op jit(solution)/shard_map/ppermute | solution.py:25
  5.2 2.2 %collective-permute-done = bf16[32,896]{1,0:T(8,128)(2,1)S(1)} collective-permute-done((bf16[32,896]{1,0:T(8,128)(2,1)S(1)}, bf16[32,896]{1,0:T(8,128)(2,1)S(1)}, u32[]{:S(2)}, u32[]{:S(2)}) %collective-permute-start) | collective-permute-done | bytes 57376 | tf_op jit(solution)/shard_map/ppermute | solution.py:25
  7.4 2.1 %collective-permute-start.1 = (bf16[32,896]{1,0:T(8,128)(2,1)S(1)}, bf16[32,896]{1,0:T(8,128)(2,1)S(1)}, u32[]{:S(2)}, u32[]{:S(2)}) collective-permute-start(bf16[32,896]{1,0:T(8,128)(2,1)S(1)} %add_convert_fusion.1), channel_id=1, source_target_pairs={{0,8},{4,12},{8,0},{12,4},{16,24},{20,28},{24,16},{28,20},{1,9},{5... | collective-permute-start | bytes 172040 | tf_op jit(solution)/shard_map/ppermute | solution.py:25
  9.5 2.2 %collective-permute-done.1 = bf16[32,896]{1,0:T(8,128)(2,1)S(1)} collective-permute-done((bf16[32,896]{1,0:T(8,128)(2,1)S(1)}, bf16[32,896]{1,0:T(8,128)(2,1)S(1)}, u32[]{:S(2)}, u32[]{:S(2)}) %collective-permute-start.1) | collective-permute-done | bytes 57376 | tf_op jit(solution)/shard_map/ppermute | solution.py:25
  11.7 3.1 %collective-permute-start.2 = (bf16[32,896]{1,0:T(8,128)(2,1)S(1)}, bf16[32,896]{1,0:T(8,128)(2,1)S(1)}, u32[]{:S(2)}, u32[]{:S(2)}) collective-permute-start(bf16[32,896]{1,0:T(8,128)(2,1)S(1)} %add_convert_fusion), channel_id=1, source_target_pairs={{0,16},{4,20},{8,24},{12,28},{16,0},{20,4},{24,8},{28,12},{1,17},{... | collective-permute-start | bytes 172040 | tf_op jit(solution)/shard_map/ppermute | solution.py:25
  14.8 0.1 pad.12.clone
  14.9 5.3 %expand_gates.1 = (f32[32,16,1280]{2,1,0:T(8,128)}, f32[32,8,128]{2,1,0:T(8,128)}) custom-call(s32[32]{0:T(128)} %lengths_ref.1, s32[1]{0:T(128)} %bitcast.4.first_ref, f32[32,8,1280]{2,1,0:T(8,128)} %cum_ref.1), custom_call_target="tpu_custom_call" | custom-call | tf_op jit(solution)/shard_map/expand_gates/pallas_call | solution.py:87
  20.2 0.0 collective-permute-done.2
  20.2 0.2 fusion.7
  20.4 0.1 fusion.3
  20.5 0.1 reshape.48
  20.6 0.1 reshape.47
  20.7 0.1 reshape.43
  20.9 0.0 copy-start.1
  20.9 12.6 %attend.1.mine_ref = bf16[32,640]{1,0:T(8,128)(2,1)S(1)} custom-call(bf16[32,16,256]{2,1,0:T(8,128)(2,1)S(1)} %fusion.2.query_ref, bf16[32,2560,128]{2,1,0:T(8,128)(2,1)} %bitcast.10, f32[32,16,1280]{2,1,0:T(8,128)} %get-tuple-element.6.bias_ref, f32[32,8,128]{2,1,0:T(8,128)} %get-tuple-element.7.last_ref), custom_call_target="tpu_custom_call" | custom-call | tf_op jit(solution)/shard_map/attend/pallas_call | solution.py:163
  33.5 1.6 %collective-permute-start.3 = (bf16[32,640]{1,0:T(8,128)(2,1)S(1)}, bf16[32,640]{1,0:T(8,128)(2,1)S(1)}, u32[]{:S(2)}, u32[]{:S(2)}) collective-permute-start(bf16[32,640]{1,0:T(8,128)(2,1)S(1)} %attend.1.mine_ref), channel_id=1, source_target_pairs={{0,4},{4,0},{8,12},{12,8},{16,20},{20,16},{24,28},{28,24},{1,5},{5... | collective-permute-start | bytes 122888 | tf_op jit(solution)/shard_map/ppermute | solution.py:25
  35.1 0.0 copy-done.1
  35.1 0.1 fusion.4
  35.2 0.2 multiply_reduce_fusion
  35.3 0.1 copy.19
  35.4 2.1 %collective-permute-done.3.other_ref = bf16[32,640]{1,0:T(8,128)(2,1)S(1)} collective-permute-done((bf16[32,640]{1,0:T(8,128)(2,1)S(1)}, bf16[32,640]{1,0:T(8,128)(2,1)S(1)}, u32[]{:S(2)}, u32[]{:S(2)}) %collective-permute-start.3) | collective-permute-done | bytes 40992 | tf_op jit(solution)/shard_map/ppermute | solution.py:25
  37.6 0.2 merge.2.mine_ref
  37.8 1.6 %collective-permute-start.4 = (bf16[32,640]{1,0:T(8,128)(2,1)S(1)}, bf16[32,640]{1,0:T(8,128)(2,1)S(1)}, u32[]{:S(2)}, u32[]{:S(2)}) collective-permute-start(bf16[32,640]{1,0:T(8,128)(2,1)S(1)} %merge.2.mine_ref), channel_id=1, source_target_pairs={{0,8},{4,12},{8,0},{12,4},{16,24},{20,28},{24,16},{28,20},{1,9},{5... | collective-permute-start | bytes 122888 | tf_op jit(solution)/shard_map/ppermute | solution.py:25
  39.4 0.1 copy.20
  39.5 2.4 %collective-permute-done.4.other_ref = bf16[32,640]{1,0:T(8,128)(2,1)S(1)} collective-permute-done((bf16[32,640]{1,0:T(8,128)(2,1)S(1)}, bf16[32,640]{1,0:T(8,128)(2,1)S(1)}, u32[]{:S(2)}, u32[]{:S(2)}) %collective-permute-start.4) | collective-permute-done | bytes 40992 | tf_op jit(solution)/shard_map/ppermute | solution.py:25
  41.9 0.2 merge.3.mine_ref
  42.1 0.1 collective-permute-start.5
  42.2 0.1 maximum_maximum_fusion.fresh_ref
  42.2 0.1 broadcast_in_dim.12
  42.4 0.1 reshape.46.value_ref
  42.5 4.6 %collective-permute-done.5.other_ref = bf16[32,640]{1,0:T(8,128)(2,1)S(1)} collective-permute-done((bf16[32,640]{1,0:T(8,128)(2,1)S(1)}, bf16[32,640]{1,0:T(8,128)(2,1)S(1)}, u32[]{:S(2)}, u32[]{:S(2)}) %collective-permute-start.5) | collective-permute-done | bytes 40992 | tf_op jit(solution)/shard_map/ppermute | solution.py:25
  47.0 0.3 finish.1
  47.3 0.0 copy-done
  47.3 0.2 convolution_convert_fusion
  47.5 0.0 collective-permute-start.6
  47.5 1.2 %collective-permute-done.6 = bf16[32,512]{1,0:T(8,128)(2,1)S(1)} collective-permute-done((bf16[32,512]{1,0:T(8,128)(2,1)S(1)}, bf16[32,512]{1,0:T(8,128)(2,1)S(1)}, u32[]{:S(2)}, u32[]{:S(2)}) %collective-permute-start.6) | collective-permute-done | bytes 32800 | tf_op jit(solution)/shard_map/ppermute | solution.py:25
  48.8 1.5 %collective-permute-start.7 = (bf16[32,512]{1,0:T(8,128)(2,1)S(1)}, bf16[32,512]{1,0:T(8,128)(2,1)S(1)}, u32[]{:S(2)}, u32[]{:S(2)}) collective-permute-start(bf16[32,512]{1,0:T(8,128)(2,1)S(1)} %add_convert_fusion.3), channel_id=1, source_target_pairs={{0,2},{1,3},{2,0},{3,1},{4,6},{5,7},{6,4},{7,5},{8,10},{9,11},{10,... | collective-permute-start | bytes 98312 | tf_op jit(solution)/shard_map/ppermute | solution.py:25
  50.3 0.7 %copy.21 = f32[32,8]{0,1:T(8,128)} copy(f32[32,8]{1,0:T(8,128)S(1)} %bitcast.9) | data formatting | bytes 2048
  51.0 1.8 %collective-permute-done.7 = bf16[32,512]{1,0:T(8,128)(2,1)S(1)} collective-permute-done((bf16[32,512]{1,0:T(8,128)(2,1)S(1)}, bf16[32,512]{1,0:T(8,128)(2,1)S(1)}, u32[]{:S(2)}, u32[]{:S(2)}) %collective-permute-start.7) | collective-permute-done | bytes 32800 | tf_op jit(solution)/shard_map/ppermute | solution.py:25
  52.7 0.6 %add_convert_fusion.2 = bf16[32,512]{1,0:T(8,128)(2,1)} fusion(bf16[32,512]{1,0:T(8,128)(2,1)S(1)} %collective-permute-done.7, bf16[32,512]{1,0:T(8,128)(2,1)S(1)} %add_convert_fusion.3), kind=kLoop, calls=%fused_computation.12 | loop fusion | flops 65536 | bytes 98304 | tf_op jit(solution)/shard_map/convert_element_type | solution.py:425
  (10 shorter events, 0.1 us)
Async XLA Ops:
  0.6 46.7 %copy-start = (bf16[512,512]{1,0:T(8,128)(2,1)S(1)}, bf16[512,512]{1,0:T(8,128)(2,1)}, u32[]{:S(2)}) copy-start(bf16[512,512]{1,0:T(8,128)(2,1)} %param.21) | copy-start | bytes 1572868
  2.1 5.2 %collective-permute-start = (bf16[32,896]{1,0:T(8,128)(2,1)S(1)}, bf16[32,896]{1,0:T(8,128)(2,1)S(1)}, u32[]{:S(2)}, u32[]{:S(2)}) collective-permute-start(bf16[32,896]{1,0:T(8,128)(2,1)S(1)} %project.1), channel_id=1, source_target_pairs={{0,4},{4,0},{8,12},{12,8},{16,20},{20,16},{24,28},{28,24},{1,5},{5... | collective-permute-start | bytes 172040 | tf_op jit(solution)/shard_map/ppermute | solution.py:25
  7.4 4.3 %collective-permute-start.1 = (bf16[32,896]{1,0:T(8,128)(2,1)S(1)}, bf16[32,896]{1,0:T(8,128)(2,1)S(1)}, u32[]{:S(2)}, u32[]{:S(2)}) collective-permute-start(bf16[32,896]{1,0:T(8,128)(2,1)S(1)} %add_convert_fusion.1), channel_id=1, source_target_pairs={{0,8},{4,12},{8,0},{12,4},{16,24},{20,28},{24,16},{28,20},{1,9},{5... | collective-permute-start | bytes 172040 | tf_op jit(solution)/shard_map/ppermute | solution.py:25
  11.7 8.5 %collective-permute-start.2 = (bf16[32,896]{1,0:T(8,128)(2,1)S(1)}, bf16[32,896]{1,0:T(8,128)(2,1)S(1)}, u32[]{:S(2)}, u32[]{:S(2)}) collective-permute-start(bf16[32,896]{1,0:T(8,128)(2,1)S(1)} %add_convert_fusion), channel_id=1, source_target_pairs={{0,16},{4,20},{8,24},{12,28},{16,0},{20,4},{24,8},{28,12},{1,17},{... | collective-permute-start | bytes 172040 | tf_op jit(solution)/shard_map/ppermute | solution.py:25
  20.9 14.2 %copy-start.1 = (f32[8]{0:T(128)S(1)}, f32[8]{0:T(128)}, u32[]{:S(2)}) copy-start(f32[8]{0:T(128)} %param.17) | copy-start | bytes 100
  33.5 4.1 %collective-permute-start.3 = (bf16[32,640]{1,0:T(8,128)(2,1)S(1)}, bf16[32,640]{1,0:T(8,128)(2,1)S(1)}, u32[]{:S(2)}, u32[]{:S(2)}) collective-permute-start(bf16[32,640]{1,0:T(8,128)(2,1)S(1)} %attend.1.mine_ref), channel_id=1, source_target_pairs={{0,4},{4,0},{8,12},{12,8},{16,20},{20,16},{24,28},{28,24},{1,5},{5... | collective-permute-start | bytes 122888 | tf_op jit(solution)/shard_map/ppermute | solution.py:25
  37.8 4.1 %collective-permute-start.4 = (bf16[32,640]{1,0:T(8,128)(2,1)S(1)}, bf16[32,640]{1,0:T(8,128)(2,1)S(1)}, u32[]{:S(2)}, u32[]{:S(2)}) collective-permute-start(bf16[32,640]{1,0:T(8,128)(2,1)S(1)} %merge.2.mine_ref), channel_id=1, source_target_pairs={{0,8},{4,12},{8,0},{12,4},{16,24},{20,28},{24,16},{28,20},{1,9},{5... | collective-permute-start | bytes 122888 | tf_op jit(solution)/shard_map/ppermute | solution.py:25
  42.1 5.0 %collective-permute-start.5 = (bf16[32,640]{1,0:T(8,128)(2,1)S(1)}, bf16[32,640]{1,0:T(8,128)(2,1)S(1)}, u32[]{:S(2)}, u32[]{:S(2)}) collective-permute-start(bf16[32,640]{1,0:T(8,128)(2,1)S(1)} %merge.3.mine_ref), channel_id=1, source_target_pairs={{0,16},{4,20},{8,24},{12,28},{16,0},{20,4},{24,8},{28,12},{1,17},{... | collective-permute-start | bytes 122888 | tf_op jit(solution)/shard_map/ppermute | solution.py:25
  47.5 1.2 %collective-permute-start.6 = (bf16[32,512]{1,0:T(8,128)(2,1)S(1)}, bf16[32,512]{1,0:T(8,128)(2,1)S(1)}, u32[]{:S(2)}, u32[]{:S(2)}) collective-permute-start(bf16[32,512]{1,0:T(8,128)(2,1)S(1)} %convolution_convert_fusion), channel_id=1, source_target_pairs={{0,1},{1,0},{2,3},{3,2},{4,5},{5,4},{6,7},{7,6},{8,9},{9,8},{10,11... | collective-permute-start | bytes 98312 | tf_op jit(solution)/shard_map/ppermute | solution.py:25
  48.8 4.0 %collective-permute-start.7 = (bf16[32,512]{1,0:T(8,128)(2,1)S(1)}, bf16[32,512]{1,0:T(8,128)(2,1)S(1)}, u32[]{:S(2)}, u32[]{:S(2)}) collective-permute-start(bf16[32,512]{1,0:T(8,128)(2,1)S(1)} %add_convert_fusion.3), channel_id=1, source_target_pairs={{0,2},{1,3},{2,0},{3,1},{4,6},{5,7},{6,4},{7,5},{8,10},{9,11},{10,... | collective-permute-start | bytes 98312 | tf_op jit(solution)/shard_map/ppermute | solution.py:25
